TPU v7x, 128 devices: a whole 4x4x4 slice. The times are simulated.
128 devices in a mesh: st: 64 (over z, y, x), tp: 2 (over core).
Axes of the slice: x: 4, y: 4, z: 4, core: 2. Of those that a mesh axis runs over, the one named last changes fastest.
Arguments:
- hidden: bfloat16 [32768, 2048], P('st'), may hold values from -24 to 24
- passage_store: bfloat16 [2048, 64, 2048], P('st'), may hold values from -6 to 6
- passage_ids: int32 [512, 4], P('st'), may hold values from 0 to 2047, as said below
- query_weight: bfloat16 [2048, 512], P(None, 'tp'), may hold values from -0.125 to 0.125
- gate_weight: bfloat16 [2048, 512], P(None, 'tp'), may hold values from -0.125 to 0.125
- key_weight: bfloat16 [2048, 512], P(None, 'tp'), may hold values from -0.125 to 0.125
- value_weight: bfloat16 [2048, 512], P(None, 'tp'), may hold values from -0.125 to 0.125
- output_grad: bfloat16 [32768, 512], P('st', 'tp'), may hold values from -6 to 6
Outputs:
- grad_hidden: bfloat16 [32768, 2048], P(('st', 'tp'))
- grad_store: bfloat16 [2048, 64, 2048], P(('st', 'tp'))
- grad_value_weight: float32 [2048, 512], P(None, 'tp')
Inputs may be any that keep to these rules, and one draw needn't show every extreme that they name: `passage_ids`: passage p is held at st index p // 32. The 32 ids of one index of st (its 8 blocks) are distinct; at most 1 of them name passages of one owner, and on every index some owner is named exactly 1 times. Every index reads at least one passage of the owner before it, of the owner after it and of the owner half the axis away.
All inputs are finite; a program needn't handle non-finite values.
Results may differ from a plain program's by a relative error of at most 0.012.
The roundings to bfloat16 on the way count: a program that leaves them out, or rounds other values in their place, can miss the bound.
Values may be sent and summed in bfloat16 or wider, within the bound.
No kernel may reach another device: no remote copies, remote signals or barrier semaphores. Data moves between devices by JAX's collectives and lax.ppermute only.
A program may use at most 128 MiB of HBM per device.

v0:
```python
import jax
import jax.numpy as jnp
from jax import lax
from jax.sharding import PartitionSpec as P

HEAD_DIM = 256


def joined_along(blocks, dim):
    dims = list(blocks.shape[1:])
    dims[dim] *= blocks.shape[0]
    return jnp.moveaxis(blocks, 0, dim).reshape(dims)


def copy_for_each(x, axis):
    copies = jnp.broadcast_to(x, (lax.axis_size(axis), *x.shape))
    return lax.all_to_all(copies, axis, split_axis=0, concat_axis=0, tiled=True)


def gather_directly(x, axis, dim):
    return joined_along(copy_for_each(x, axis), dim)


def body(
    hidden,
    passage_store,
    passage_ids,
    query_weight,
    gate_weight,
    key_weight,
    value_weight,
    output_grad,
):
    owner_count = lax.axis_size("st")
    own_index = lax.axis_index("st")
    held_count = passage_store.shape[0]
    span_rows = passage_store.shape[1]
    model_width = passage_store.shape[2]
    block_count = passage_ids.shape[0]
    per_block = passage_ids.shape[1]
    requests = block_count * per_block
    capacity = max(1, 2 * requests // owner_count)
    local_width = query_weight.shape[1]
    local_heads = local_width // HEAD_DIM
    tokens_here = hidden.shape[0]
    block_rows = tokens_here // block_count
    all_ids = gather_directly(passage_ids, "st", 0).reshape(owner_count, requests)
    owner_of = all_ids // held_count
    local_index = all_ids % held_count
    positions = jnp.arange(requests, dtype=jnp.int32)
    earlier = positions[None, :] < positions[:, None]
    matching = owner_of[:, :, None] == owner_of[:, None, :]
    slot_rank = jnp.sum(matching & earlier[None], axis=2)
    slot_iota = jnp.arange(capacity, dtype=jnp.int32)
    placed = (owner_of == own_index)[:, :, None] & (
        slot_rank[:, :, None] == slot_iota[None, None, :]
    )
    slot_table = jnp.sum(jnp.where(placed, local_index[:, :, None], 0), axis=1)
    filled = jnp.any(placed, axis=1)
    my_owner = lax.dynamic_index_in_dim(owner_of, own_index, 0, keepdims=False)
    my_rank = lax.dynamic_index_in_dim(slot_rank, own_index, 0, keepdims=False)
    slot_flat = my_owner * capacity + my_rank
    store_rows = passage_store.reshape(held_count * span_rows, model_width)
    keys_here = (
        jnp.dot(store_rows, key_weight, preferred_element_type=jnp.float32)
        .astype(jnp.bfloat16)
        .reshape(held_count, span_rows, local_width)
    )
    values_here = (
        jnp.dot(store_rows, value_weight, preferred_element_type=jnp.float32)
        .astype(jnp.bfloat16)
        .reshape(held_count, span_rows, local_width)
    )
    came_keys, came_values = (
        lax.all_to_all(keys_here[slot_table], "st", split_axis=0, concat_axis=0, tiled=True),
        lax.all_to_all(values_here[slot_table], "st", split_axis=0, concat_axis=0, tiled=True),
    )
    got_keys = came_keys.reshape(owner_count * capacity, span_rows, local_width)[slot_flat]
    got_values = came_values.reshape(owner_count * capacity, span_rows, local_width)[slot_flat]
    key_heads = got_keys.reshape(block_count, per_block * span_rows, local_heads, HEAD_DIM)
    value_heads = got_values.reshape(block_count, per_block * span_rows, local_heads, HEAD_DIM)
    queries = jnp.dot(hidden, query_weight, preferred_element_type=jnp.float32).astype(jnp.bfloat16)
    gates = jnp.dot(hidden, gate_weight, preferred_element_type=jnp.float32)
    query_heads = queries.reshape(block_count, block_rows, local_heads, HEAD_DIM)
    score_scale = HEAD_DIM ** (-0.5)
    scores = (
        jnp.einsum("bqhd,bkhd->bhqk", query_heads, key_heads, preferred_element_type=jnp.float32)
        * score_scale
    )
    probs = jax.nn.softmax(scores, axis=-1)
    probs_low = probs.astype(jnp.bfloat16)
    attended = jnp.einsum(
        "bhqk,bkhd->bqhd", probs_low, value_heads, preferred_element_type=jnp.float32
    ).reshape(tokens_here, local_width)
    gate_sigmoid = jax.nn.sigmoid(gates)
    upstream = output_grad.astype(jnp.float32)
    d_attended = (upstream * gates * gate_sigmoid).astype(jnp.bfloat16)
    d_gates = (upstream * attended * gate_sigmoid * (1.0 + gates * (1.0 - gate_sigmoid))).astype(
        jnp.bfloat16
    )
    d_heads = d_attended.reshape(block_count, block_rows, local_heads, HEAD_DIM)
    d_probs = jnp.einsum(
        "bqhd,bkhd->bhqk", d_heads, value_heads, preferred_element_type=jnp.float32
    )
    centre = jnp.sum(probs * d_probs, axis=-1, keepdims=True)
    d_scores = (probs * (d_probs - centre) * score_scale).astype(jnp.bfloat16)
    d_queries = (
        jnp.einsum("bhqk,bkhd->bqhd", d_scores, key_heads, preferred_element_type=jnp.float32)
        .astype(jnp.bfloat16)
        .reshape(tokens_here, local_width)
    )
    d_block_keys = jnp.einsum(
        "bhqk,bqhd->bkhd", d_scores, query_heads, preferred_element_type=jnp.float32
    ).reshape(requests, span_rows, local_width)
    d_block_values = jnp.einsum(
        "bhqk,bqhd->bkhd", probs_low, d_heads, preferred_element_type=jnp.float32
    ).reshape(requests, span_rows, local_width)
    contract = (((1,), (1,)), ((), ()))
    slot_total = owner_count * capacity
    back_keys = (
        jnp.zeros((slot_total, span_rows, local_width), jnp.float32).at[slot_flat].set(d_block_keys)
    )
    back_values = (
        jnp.zeros((slot_total, span_rows, local_width), jnp.float32)
        .at[slot_flat]
        .set(d_block_values)
    )
    came_dkeys, came_dvalues = (
        lax.all_to_all(
            back_keys.reshape(owner_count, capacity, span_rows, local_width).astype(jnp.bfloat16),
            "st",
            split_axis=0,
            concat_axis=0,
            tiled=True,
        ).astype(jnp.float32),
        lax.all_to_all(
            back_values.reshape(owner_count, capacity, span_rows, local_width).astype(jnp.bfloat16),
            "st",
            split_axis=0,
            concat_axis=0,
            tiled=True,
        ).astype(jnp.float32),
    )
    slot_owner = jnp.where(filled, slot_table, -1).reshape(slot_total)
    selector = (jnp.arange(held_count, dtype=jnp.int32)[:, None] == slot_owner[None, :]).astype(
        jnp.float32
    )
    key_totals = jnp.dot(
        selector,
        came_dkeys.reshape(slot_total, span_rows * local_width),
        precision=lax.Precision.HIGHEST,
        preferred_element_type=jnp.float32,
    )
    value_totals = jnp.dot(
        selector,
        came_dvalues.reshape(slot_total, span_rows * local_width),
        precision=lax.Precision.HIGHEST,
        preferred_element_type=jnp.float32,
    )
    key_low = key_totals.astype(jnp.bfloat16).reshape(held_count, span_rows, local_width)
    value_low = value_totals.astype(jnp.bfloat16).reshape(held_count, span_rows, local_width)
    weight_part = lax.dot_general(
        store_rows,
        value_low.reshape(held_count * span_rows, local_width),
        (((0,), (0,)), ((), ())),
        preferred_element_type=jnp.float32,
    )
    grad_value_weight = lax.psum(weight_part, "st")
    full_query, full_gate, full_key, full_value = (
        lax.all_gather(query_weight, "tp", axis=1, tiled=True),
        lax.all_gather(gate_weight, "tp", axis=1, tiled=True),
        lax.all_gather(key_weight, "tp", axis=1, tiled=True),
        lax.all_gather(value_weight, "tp", axis=1, tiled=True),
    )
    my_dqueries, my_dgates = (
        lax.all_to_all(d_queries, "tp", split_axis=0, concat_axis=1, tiled=True),
        lax.all_to_all(d_gates, "tp", split_axis=0, concat_axis=1, tiled=True),
    )
    grad_hidden = (
        lax.dot_general(my_dqueries, full_query, contract, preferred_element_type=jnp.float32)
        + lax.dot_general(my_dgates, full_gate, contract, preferred_element_type=jnp.float32)
    ).astype(jnp.bfloat16)
    my_keys, my_values = (
        lax.all_to_all(key_low, "tp", split_axis=0, concat_axis=2, tiled=True),
        lax.all_to_all(value_low, "tp", split_axis=0, concat_axis=2, tiled=True),
    )
    my_count = my_keys.shape[0]
    full_width = my_keys.shape[2]
    summed = lax.dot_general(
        my_keys.reshape(my_count * span_rows, full_width),
        full_key,
        contract,
        preferred_element_type=jnp.float32,
    ) + lax.dot_general(
        my_values.reshape(my_count * span_rows, full_width),
        full_value,
        contract,
        preferred_element_type=jnp.float32,
    )
    grad_store = summed.reshape(my_count, span_rows, model_width).astype(jnp.bfloat16)
    return (grad_hidden, grad_store, grad_value_weight)


def solution(mesh):
    placed = (
        P("st", None),
        P("st", None, None),
        P("st", None),
        P(None, "tp"),
        P(None, "tp"),
        P(None, "tp"),
        P(None, "tp"),
        P("st", "tp"),
    )
    return jax.shard_map(
        body,
        mesh=mesh,
        in_specs=placed,
        out_specs=(P(("st", "tp"), None), P(("st", "tp"), None, None), P(None, "tp")),
        check_vma=False,
    )
```

profile of v0, /device:TPU:0, one launch (start us, length us, event | category | flops | bytes accessed | tf_op | source)
XLA Modules:
  0.0 345.5 jit_solution(16902328177386462916)
XLA Ops:
  8.1 0.7 all-gather.5.cloned.1.call-update
  8.7 1.4 broadcast_in_dim.6
  10.1 11.5 %all-to-all-start = ((s32[64,8,4]{1,2,0:T(4,128)}), s32[64,8,4]{1,2,0:T(4,128)S(1)}, u32[]{:S(2)}, u32[]{:S(2)}) async-start(s32[64,8,4]{1,2,0:T(4,128)} %broadcast_in_dim.6), calls=%async_computation | async-start | bytes 262144 | tf_op jit(solution)/shard_map/all_to_all | solution.py:17
  21.6 6.8 %convolution_convert_fusion.2 = bf16[2048,256]{1,0:T(8,128)(2,1)S(1)} fusion(bf16[2048,2048]{1,0:T(8,128)(2,1)} %bitcast.113, bf16[2048,256]{1,0:T(8,128)(2,1)} %param.14), kind=kOutput, calls=%fused_computation.14 | convolution fusion | flops 2148007936 | bytes 10485760 | tf_op jit(solution)/shard_map/dot_general | solution.py:70
  28.4 3.1 all-to-all-done
  31.7 0.2 convert_reduce_fusion
  32.1 2.0 gather_fusion.2
  34.1 7.5 %all-to-all-start.2 = ((bf16[64,1,64,256]{3,2,1,0:T(8,128)(2,1)}), bf16[64,1,64,256]{3,2,1,0:T(8,128)(2,1)}, u32[]{:S(2)}, u32[]{:S(2)}) async-start(bf16[64,1,64,256]{3,2,1,0:T(8,128)(2,1)} %bitcast.120), calls=%async_computation.2 | async-start | bytes 4194304 | tf_op jit(solution)/shard_map/all_to_all | solution.py:76
  41.6 0.7 all-gather.7.cloned.1.call-update
  42.3 6.0 %convolution_convert_fusion.3 = bf16[2048,256]{1,0:T(8,128)(2,1)S(1)} fusion(bf16[2048,2048]{1,0:T(8,128)(2,1)} %bitcast.114, bf16[2048,256]{1,0:T(8,128)(2,1)} %param.13), kind=kOutput, calls=%fused_computation.15 | convolution fusion | flops 2148007936 | bytes 10485760 | tf_op jit(solution)/shard_map/dot_general | solution.py:65
  48.3 2.0 gather_fusion
  50.3 20.6 %all-to-all-done.2 = bf16[64,1,64,256]{3,2,1,0:T(8,128)(2,1)} async-done(((bf16[64,1,64,256]{3,2,1,0:T(8,128)(2,1)}), bf16[64,1,64,256]{3,2,1,0:T(8,128)(2,1)}, u32[]{:S(2)}, u32[]{:S(2)}) %all-to-all-start.2) | async-done | bytes 2097184 | tf_op jit(solution)/shard_map/all_to_all | solution.py:76
  70.9 6.3 %all-to-all-start.1 = ((bf16[64,1,64,256]{3,2,1,0:T(8,128)(2,1)}), bf16[64,1,64,256]{3,2,1,0:T(8,128)(2,1)}, u32[]{:S(2)}, u32[]{:S(2)}) async-start(bf16[64,1,64,256]{3,2,1,0:T(8,128)(2,1)} %bitcast.119), calls=%async_computation.1 | async-start | bytes 4194304 | tf_op jit(solution)/shard_map/all_to_all | solution.py:75
  77.2 0.2 all-gather.9.cloned.1.call-start
  77.5 0.5 all-gather.9.cloned.1.call-update
  78.0 0.7 convolution_convert_fusion.5
  78.7 0.2 add_reduce_fusion
  78.9 2.2 gather_fusion.3
  81.1 25.6 %all-to-all-done.1 = bf16[64,1,64,256]{3,2,1,0:T(8,128)(2,1)} async-done(((bf16[64,1,64,256]{3,2,1,0:T(8,128)(2,1)}), bf16[64,1,64,256]{3,2,1,0:T(8,128)(2,1)}, u32[]{:S(2)}, u32[]{:S(2)}) %all-to-all-start.1) | async-done | bytes 2097184 | tf_op jit(solution)/shard_map/all_to_all | solution.py:75
  106.8 3.2 gather_fusion.1
  109.9 1.7 convolution_multiply_fusion
  111.6 0.8 copy-done.2
  112.4 0.9 fusion.42
  113.3 3.0 fusion.23
  116.3 3.0 fusion.18
  119.3 0.4 fusion.43
  119.8 4.3 %convolution_convert_fusion.4 = bf16[8,256,64]{1,2,0:T(8,128)(2,1)S(1)} fusion(bf16[8,256,256]{2,1,0:T(8,128)(2,1)} %bitcast.126, f32[8,64,256]{2,1,0:T(8,128)S(1)} %fusion.43, f32[8,64,256]{2,1,0:T(8,128)} %get-tuple-element.26, f32[8,64]{1,0:T(8,128)S(1)} %get-tuple-element.25), kind=kOutput, calls=%fused_computation.25 | convolution fusion | flops 68158208 | bytes 2361344 | tf_op jit(solution)/shard_map/bhqk,bkhd->bqhd/dot_general | solution.py:108
  124.2 0.8 copy.60
  125.0 3.4 all-to-all-start.4
  128.5 2.5 fusion.21
  131.0 2.5 broadcast.196.clone.1
  133.6 5.3 %scatter_fusion.1 = f32[64,64,256]{2,1,0:T(8,128)} fusion(f32[64,64,256]{2,1,0:T(8,128)} %broadcast.196.clone.1, s32[32]{0:T(128)S(1)} %fusion.35, f32[32,64,256]{2,1,0:T(8,128)S(1)} %bitcast.117), kind=kCustom, calls=%fused_computation.5 | custom fusion | bytes 6291584 | tf_op jit(solution)/shard_map/scatter | solution.py:126
  138.9 3.8 %convert_bitcast_fusion = bf16[64,1,64,256]{3,2,1,0:T(8,128)(2,1)} fusion(f32[64,64,256]{2,1,0:T(8,128)} %scatter_fusion.1), kind=kLoop, calls=%fused_computation.16 | loop fusion | flops 1048576 | bytes 6291456 | tf_op jit(solution)/shard_map/convert_element_type | solution.py:137
  142.7 3.9 %all_to_all.93 = bf16[2,256,256]{1,2,0:T(8,128)(2,1)S(1)} all-to-all(bf16[2,256,256]{1,2,0:T(8,128)(2,1)S(1)} %copy.59), channel_id=1, replica_groups=mesh['st'=64,'tp'=2] {'tp'}, dimensions={0} | all-to-all | bytes 524288 | tf_op jit(solution)/shard_map/all_to_all | solution.py:176
  146.7 6.0 %all-to-all-start.7 = ((bf16[64,1,64,256]{3,2,1,0:T(8,128)(2,1)}), bf16[64,1,64,256]{3,2,1,0:T(8,128)(2,1)S(1)}, u32[]{:S(2)}, u32[]{:S(2)}) async-start(bf16[64,1,64,256]{3,2,1,0:T(8,128)(2,1)} %convert_bitcast_fusion), calls=%async_computation.7 | async-start | bytes 4194304 | tf_op jit(solution)/shard_map/all_to_all | solution.py:136
  152.7 0.5 all-gather.11.cloned.1.call-update
  153.3 6.0 %fusion.9 = f32[8,256,256]{1,2,0:T(8,128)} fusion(bf16[8,64,256]{2,1,0:T(8,128)(2,1)S(1)} %bitcast.144, f32[8,64,256]{2,1,0:T(8,128)} %copy-done.4, f32[8,64,256]{2,1,0:T(8,128)} %get-tuple-element.26, f32[8,64]{1,0:T(8,128)S(1)} %get-tuple-element.25), kind=kOutput, calls=%fused_computation.27 | convolution fusion | flops 68027136 | bytes 3409920 | tf_op jit(solution)/shard_map/bhqk,bqhd->bkhd/dot_general | solution.py:112
  159.3 2.5 broadcast.196.clone
  161.8 6.5 %scatter_fusion = f32[64,64,256]{2,1,0:T(8,128)} fusion(f32[64,64,256]{2,1,0:T(8,128)} %broadcast.196.clone, s32[32]{0:T(128)S(1)} %fusion.35, f32[32,64,256]{2,1,0:T(8,128)} %bitcast.136), kind=kCustom, calls=%fused_computation.4 | custom fusion | bytes 6291584 | tf_op jit(solution)/shard_map/scatter | solution.py:121
  168.3 3.8 %convert_bitcast_fusion.1 = bf16[64,1,64,256]{3,2,1,0:T(8,128)(2,1)} fusion(f32[64,64,256]{2,1,0:T(8,128)} %scatter_fusion), kind=kLoop, calls=%fused_computation.17 | loop fusion | flops 1048576 | bytes 6291456 | tf_op jit(solution)/shard_map/convert_element_type | solution.py:130
  172.1 11.0 %all-to-all-done.7 = bf16[64,1,64,256]{3,2,1,0:T(8,128)(2,1)S(1)} async-done(((bf16[64,1,64,256]{3,2,1,0:T(8,128)(2,1)}), bf16[64,1,64,256]{3,2,1,0:T(8,128)(2,1)S(1)}, u32[]{:S(2)}, u32[]{:S(2)}) %all-to-all-start.7) | async-done | bytes 2097184 | tf_op jit(solution)/shard_map/all_to_all | solution.py:136
  183.1 6.0 %all-to-all-start.5 = ((bf16[64,1,64,256]{3,2,1,0:T(8,128)(2,1)}), bf16[64,1,64,256]{3,2,1,0:T(8,128)(2,1)}, u32[]{:S(2)}, u32[]{:S(2)}) async-start(bf16[64,1,64,256]{3,2,1,0:T(8,128)(2,1)} %convert_bitcast_fusion.1), calls=%async_computation.5 | async-start | bytes 4194304 | tf_op jit(solution)/shard_map/all_to_all | solution.py:129
  189.1 0.3 all-reduce.2.cloned.1.call-start
  189.3 1.3 copy.68
  190.6 0.4 convolution_convert_fusion
  191.1 0.5 reshape_reshape.7
  191.6 7.1 %convolution_bitcast_fusion = f32[2048,256]{0,1:T(8,128)} fusion(bf16[2048,256]{1,0:T(8,128)(2,1)S(1)} %reshape_reshape.7, bf16[2048,2048]{1,0:T(8,128)(2,1)} %bitcast.115), kind=kOutput, calls=%fused_computation.11 | convolution fusion | flops 2147483648 | bytes 11534336 | tf_op jit(solution)/shard_map/dot_general | solution.py:162
  198.7 3.7 %fusion.44 = f32[256,2048]{1,0:T(8,128)} fusion(bf16[256,512]{0,1:T(8,128)(2,1)S(1)} %bitcast.139, bf16[2048,512]{1,0:T(8,128)(2,1)} %all-gather.5.cloned.1.call-done), kind=kOutput, calls=%fused_computation.86 | convolution fusion | flops 536870912 | bytes 4456448 | tf_op jit(solution)/shard_map/dot_general | solution.py:180
  202.4 4.0 %fusion.2 = bf16[256,2048]{1,0:T(8,128)(2,1)} fusion(f32[256,2048]{1,0:T(8,128)} %fusion.44, bf16[256,512]{0,1:T(8,128)(2,1)S(1)} %bitcast.142, bf16[2048,512]{1,0:T(8,128)(2,1)} %all-gather.7.cloned.1.call-done), kind=kOutput, calls=%fused_computation.13 | convolution fusion | flops 537919488 | bytes 5505024 | tf_op jit(solution)/shard_map/dot_general | solution.py:181
  206.3 14.4 %all-to-all-done.5 = bf16[64,1,64,256]{3,2,1,0:T(8,128)(2,1)} async-done(((bf16[64,1,64,256]{3,2,1,0:T(8,128)(2,1)}), bf16[64,1,64,256]{3,2,1,0:T(8,128)(2,1)}, u32[]{:S(2)}, u32[]{:S(2)}) %all-to-all-start.5) | async-done | bytes 2097184 | tf_op jit(solution)/shard_map/all_to_all | solution.py:129
  220.7 2.9 copy.65
  223.6 0.4 convolution_convert_fusion.1
  224.0 0.2 copy.66
  224.2 4.6 %all_to_all.94 = bf16[32,64,256]{2,1,0:T(8,128)(2,1)S(1)} all-to-all(bf16[32,64,256]{2,1,0:T(8,128)(2,1)S(1)} %bitcast.130), channel_id=1, replica_groups=mesh['st'=64,'tp'=2] {'tp'}, dimensions={0} | all-to-all | bytes 2097152 | tf_op jit(solution)/shard_map/all_to_all | solution.py:184
  228.8 1.1 copy.61
  229.9 0.2 copy.67
  230.1 0.2 copy.69
  230.4 4.6 %all_to_all.95 = bf16[32,64,256]{2,1,0:T(8,128)(2,1)S(1)} all-to-all(bf16[32,64,256]{2,1,0:T(8,128)(2,1)S(1)} %bitcast.133), channel_id=1, replica_groups=mesh['st'=64,'tp'=2] {'tp'}, dimensions={0} | all-to-all | bytes 2097152 | tf_op jit(solution)/shard_map/all_to_all | solution.py:185
  235.0 1.1 copy.63
  236.0 1.2 copy.70
  237.3 7.2 %fusion.45 = f32[1024,2048]{1,0:T(8,128)} fusion(bf16[1024,512]{1,0:T(8,128)(2,1)S(1)} %bitcast.140, bf16[2048,512]{1,0:T(8,128)(2,1)} %all-gather.9.cloned.1.call-done), kind=kOutput, calls=%fused_computation.87 | convolution fusion | flops 2147483648 | bytes 11534336 | tf_op jit(solution)/shard_map/dot_general | solution.py:189
  244.4 8.9 %add_convert_fusion = bf16[1024,2048]{1,0:T(8,128)(2,1)} fusion(f32[1024,2048]{1,0:T(8,128)} %fusion.45, bf16[1024,512]{1,0:T(8,128)(2,1)} %bitcast.141, bf16[2048,512]{1,0:T(8,128)(2,1)} %all-gather.11.cloned.1.call-done), kind=kOutput, calls=%fused_computation.10 | convolution fusion | flops 2151677952 | bytes 15728640 | tf_op jit(solution)/shard_map/dot_general | solution.py:194
  253.3 82.2 %all-reduce.2.cloned.1.call-done = f32[2048,256]{0,1:T(8,128)} async-done(((f32[2048,256]{0,1:T(8,128)}), f32[2048,256]{0,1:T(8,128)}) %all-reduce.2.cloned.1.call-update) | async-done | bytes 2097168 | tf_op jit(solution)/shard_map/psum | solution.py:168
  335.5 2.9 copy.64
  (36 shorter events, 0.6 us)
Async XLA Ops:
  8.0 70.0 %copy-start = (bf16[512,2048]{1,0:T(8,128)(2,1)S(1)}, bf16[512,2048]{1,0:T(8,128)(2,1)}, u32[]{:S(2)}) copy-start(bf16[512,2048]{1,0:T(8,128)(2,1)} %param.8) | copy-start | bytes 6291460
  8.0 190.7 %all-gather.5.cloned.1.call-start = ((), (), s32[]{:S(2)}) async-start(), calls=%async_computation.9 | async-start | bytes 3145728 | tf_op jit(solution)/shard_map/all_gather | solution.py:170
  10.1 21.5 %all-to-all-start = ((s32[64,8,4]{1,2,0:T(4,128)}), s32[64,8,4]{1,2,0:T(4,128)S(1)}, u32[]{:S(2)}, u32[]{:S(2)}) async-start(s32[64,8,4]{1,2,0:T(4,128)} %broadcast_in_dim.6), calls=%async_computation | async-start | bytes 262144 | tf_op jit(solution)/shard_map/all_to_all | solution.py:17
  34.1 36.9 %all-to-all-start.2 = ((bf16[64,1,64,256]{3,2,1,0:T(8,128)(2,1)}), bf16[64,1,64,256]{3,2,1,0:T(8,128)(2,1)}, u32[]{:S(2)}, u32[]{:S(2)}) async-start(bf16[64,1,64,256]{3,2,1,0:T(8,128)(2,1)} %bitcast.120), calls=%async_computation.2 | async-start | bytes 4194304 | tf_op jit(solution)/shard_map/all_to_all | solution.py:76
  41.6 160.8 %all-gather.7.cloned.1.call-start = ((), (), s32[]{:S(2)}) async-start(), calls=%async_computation.10 | async-start | bytes 3145728 | tf_op jit(solution)/shard_map/all_gather | solution.py:171
  70.9 7.1 %copy-start.3 = (bf16[2048,256]{1,0:T(8,128)(2,1)S(1)}, bf16[2048,256]{1,0:T(8,128)(2,1)}, u32[]{:S(2)}) copy-start(bf16[2048,256]{1,0:T(8,128)(2,1)} %param.11) | copy-start | bytes 3145732
  70.9 35.8 %all-to-all-start.1 = ((bf16[64,1,64,256]{3,2,1,0:T(8,128)(2,1)}), bf16[64,1,64,256]{3,2,1,0:T(8,128)(2,1)}, u32[]{:S(2)}, u32[]{:S(2)}) async-start(bf16[64,1,64,256]{3,2,1,0:T(8,128)(2,1)} %bitcast.119), calls=%async_computation.1 | async-start | bytes 4194304 | tf_op jit(solution)/shard_map/all_to_all | solution.py:75
  77.2 160.0 %all-gather.9.cloned.1.call-start = ((), (), s32[]{:S(2)}) async-start(), calls=%async_computation.11 | async-start | bytes 3145728 | tf_op jit(solution)/shard_map/all_gather | solution.py:172
  78.7 31.2 %copy-start.5 = (bf16[512,256]{1,0:T(8,128)(2,1)}, bf16[512,256]{1,0:T(8,128)(2,1)S(1)}, u32[]{:S(2)}) copy-start(bf16[512,256]{1,0:T(8,128)(2,1)S(1)} %convolution_convert_fusion.5) | copy-start | bytes 786436
  111.6 0.8 copy-start.2
  119.7 5.3 %copy-start.4 = (f32[8,64,256]{2,1,0:T(8,128)}, f32[8,64,256]{2,1,0:T(8,128)S(1)}, u32[]{:S(2)}) copy-start(f32[8,64,256]{2,1,0:T(8,128)S(1)} %fusion.43) | copy-start | bytes 1572868
  119.7 4.4 %copy-start.7 = (bf16[512,256]{1,0:T(8,128)(2,1)S(1)}, bf16[512,256]{1,0:T(8,128)(2,1)}, u32[]{:S(2)}) copy-start(bf16[512,256]{1,0:T(8,128)(2,1)} %get-tuple-element.23) | copy-start | bytes 786436
  125.0 17.7 %all-to-all-start.4 = ((bf16[2,256,256]{1,2,0:T(8,128)(2,1)}), bf16[2,256,256]{1,2,0:T(8,128)(2,1)S(1)}, u32[]{:S(2)}, u32[]{:S(2)}) async-start(bf16[2,256,256]{1,2,0:T(8,128)(2,1)} %copy.60), calls=%async_computation.4 | async-start | bytes 524288 | tf_op jit(solution)/shard_map/all_to_all | solution.py:177
  146.7 6.6 %copy-start.6 = (bf16[512,256]{1,0:T(8,128)(2,1)S(1)}, bf16[512,256]{1,0:T(8,128)(2,1)}, u32[]{:S(2)}) copy-start(bf16[512,256]{1,0:T(8,128)(2,1)} %copy-done.5) | copy-start | bytes 786436
  146.7 36.4 %all-to-all-start.7 = ((bf16[64,1,64,256]{3,2,1,0:T(8,128)(2,1)}), bf16[64,1,64,256]{3,2,1,0:T(8,128)(2,1)S(1)}, u32[]{:S(2)}, u32[]{:S(2)}) async-start(bf16[64,1,64,256]{3,2,1,0:T(8,128)(2,1)} %convert_bitcast_fusion), calls=%async_computation.7 | async-start | bytes 4194304 | tf_op jit(solution)/shard_map/all_to_all | solution.py:136
  152.7 91.7 %all-gather.11.cloned.1.call-start = ((), (), s32[]{:S(2)}) async-start(), calls=%async_computation.12 | async-start | bytes 3145728 | tf_op jit(solution)/shard_map/all_gather | solution.py:173
  183.1 37.6 %all-to-all-start.5 = ((bf16[64,1,64,256]{3,2,1,0:T(8,128)(2,1)}), bf16[64,1,64,256]{3,2,1,0:T(8,128)(2,1)}, u32[]{:S(2)}, u32[]{:S(2)}) async-start(bf16[64,1,64,256]{3,2,1,0:T(8,128)(2,1)} %convert_bitcast_fusion.1), calls=%async_computation.5 | async-start | bytes 4194304 | tf_op jit(solution)/shard_map/all_to_all | solution.py:129
  189.1 146.5 %all-reduce.2.cloned.1.call-start = ((), (), s32[]{:S(2)}) async-start(), calls=%async_computation.13 | async-start | bytes 4194304 | tf_op jit(solution)/shard_map/psum | solution.py:168
  244.4 94.0 %copy-start.1 = (bf16[512,2048]{1,0:T(8,128)(2,1)S(1)}, bf16[512,2048]{1,0:T(8,128)(2,1)}, u32[]{:S(2)}) copy-start(bf16[512,2048]{1,0:T(8,128)(2,1)} %param.8) | copy-start | bytes 6291460
Sparse Core Ops, SparseCore 0:
  10.5 15.2 all-gather.4
  44.0 14.0 all-gather.6
  79.7 14.0 all-gather.8
  154.8 14.1 all-gather.10
Sparse Core Ops, SparseCore 1:
  198.7 136.7 all-reduce.1
where the time goes:
time: 347 us; the launch traced here: 346 us
  waiting for transfers between devices  159 us (46%)
  matrix products  65.9 us (19%)
  starting transfers between devices  41.3 us (12%)
  local copies, waits for them, and re-layouts  41.1 us (12%)
  between operations  15.5 us (4%)
  blocking collectives  13.1 us (4%)
  other arithmetic  9.19 us (3%)
    psum x1, waiting for transfers between devices, body(): grad_value_weight = lax.psum(weight_part, 'st')  82.2 us
    all_to_all x1, waiting for transfers between devices, body(): lax.all_to_all(keys_here[slot_table], 'st', split_axis=0, concat_axis=0,...  25.6 us
    all_to_all x1, waiting for transfers between devices, body(): lax.all_to_all(values_here[slot_table], 'st', split_axis=0, concat_axis=0...  20.6 us
    all_to_all x1, waiting for transfers between devices, body(): lax.all_to_all(back_keys.reshape(owner_count, capacity, span_rows, local_...  14.4 us
    all_to_all x1, starting transfers between devices, copy_for_each(): return lax.all_to_all(copies, axis, split_axis=0, concat_axis=0, tiled=True)  11.5 us
    all_to_all x1, waiting for transfers between devices, body(): lax.all_to_all(back_values.reshape(owner_count, capacity, span_rows, loca...  11 us
    unnamed x23, local copies, waits for them, and re-layouts  9.75 us
    dot_general x1, matrix products, body(): lax.dot_general(my_values.reshape(my_count * span_rows, full_width), full...  8.9 us
  transfers between devices with their start and end apart: 11, of which 6 were waited for; matrix products, arithmetic and copies ran while one was open for 33% of the time, Pallas kernels for 0%

commit v1 on v0

v1 whole, which is shorter than its diff:
```python
import functools

import jax
import jax.numpy as jnp
from jax import lax
from jax.experimental import pallas as pl
from jax.experimental.pallas import tpu as pltpu
from jax.sharding import PartitionSpec as P

HEAD_DIM = 256
F32 = jnp.float32
BF16 = jnp.bfloat16
VMEM = pl.BlockSpec(memory_space=pltpu.VMEM)
SMEM = pl.BlockSpec(memory_space=pltpu.SMEM)


def dot(a, b, ca, cb):
    return lax.dot_general(a, b, (((ca,), (cb,)), ((), ())), preferred_element_type=F32)


def swap_tp(x):
    return lax.ppermute(x, "tp", [(0, 1), (1, 0)])


def exchange(x):
    return lax.all_to_all(x, "st", split_axis=0, concat_axis=0, tiled=True)


def pick_kernel(wanted_ref, rows_ref, out_ref):
    def step(i, carry):
        out_ref[i] = rows_ref[jnp.maximum(wanted_ref[i, 0] - 1, 0)]
        return carry

    lax.fori_loop(0, out_ref.shape[0], step, 0, unroll=8)


def pick(wanted, rows):
    return pl.pallas_call(
        pick_kernel,
        out_shape=jax.ShapeDtypeStruct((wanted.shape[0], *rows.shape[1:]), rows.dtype),
        in_specs=[SMEM, VMEM],
        out_specs=VMEM,
        name="pick",
    )(wanted, rows)


def probs_kernel(held, ids_ref, q_ref, da_ref, k_ref, p_ref, dv_ref):
    blocks, per = ids_ref.shape
    rows = q_ref.shape[0] // blocks
    span = k_ref.shape[1]
    scale = HEAD_DIM**-0.5
    for b in range(blocks):
        mine = slice(b * rows, (b + 1) * rows)
        owner = [lax.div(ids_ref[b, j], held) for j in range(per)]
        k = jnp.concatenate([k_ref[o] for o in owner], axis=0)
        s = dot(q_ref[mine], k, 1, 1) * scale
        e = jnp.exp(s - jnp.max(s, axis=1, keepdims=True))
        p = e / jnp.sum(e, axis=1, keepdims=True)
        p_ref[mine] = p
        dv = dot(p.astype(BF16), da_ref[mine], 0, 0).astype(BF16)
        for j in range(per):
            dv_ref[owner[j]] = dv[j * span : (j + 1) * span]


def grads_kernel(held, ids_ref, tp_ref, q_ref, da_ref, g_ref, og_ref, p_ref, k_ref, v_ref, keep_ref, send_ref, dk_ref):
    blocks, per = ids_ref.shape
    rows = q_ref.shape[0] // blocks
    span = k_ref.shape[1]
    scale = HEAD_DIM**-0.5
    half = blocks // 2
    for n in range(blocks):
        b = lax.rem(n + half * tp_ref[0], blocks)
        mine = pl.ds(pl.multiple_of(b * rows, rows), rows)
        owner = [lax.div(ids_ref[b, j], held) for j in range(per)]
        k = jnp.concatenate([k_ref[o] for o in owner], axis=0)
        v = jnp.concatenate([v_ref[o] for o in owner], axis=0)
        p = p_ref[mine]
        q = q_ref[mine]
        g = g_ref[mine]
        dp = dot(da_ref[mine], v, 1, 1)
        attended = dot(p.astype(BF16), v, 1, 0)
        centre = jnp.sum(p * dp, axis=1, keepdims=True)
        ds = (p * (dp - centre) * scale).astype(BF16)
        dq = dot(ds, k, 1, 0).astype(BF16)
        dk = dot(ds, q, 0, 0).astype(BF16)
        sg = jax.nn.sigmoid(g)
        dg = (og_ref[mine].astype(F32) * attended * sg * (1.0 + g * (1.0 - sg))).astype(BF16)
        for j in range(per):
            dk_ref[owner[j], 0:span] = dk[j * span : (j + 1) * span]
        out = keep_ref if n < half else send_ref
        at = slice((n % half) * rows, (n % half + 1) * rows)
        out[0, at] = dq
        out[1, at] = dg


def add_slots(wanted_ref, tp_ref, came_ref, acc, keep_ref, send_ref):
    span = acc.shape[1]
    acc[...] = jnp.zeros_like(acc)

    def step(i, carry):
        at = wanted_ref[i, 0]
        acc[at] = acc[at] + came_ref[i, 0:span].astype(F32)
        return carry

    lax.fori_loop(0, came_ref.shape[0], step, 0, unroll=8)
    half = keep_ref.shape[0]
    tp = tp_ref[0]
    keep_ref[...] = acc[pl.ds(1 + half * tp, half)].astype(BF16)
    send_ref[...] = acc[pl.ds(1 + half * (1 - tp), half)].astype(BF16)


def value_totals_kernel(wanted_ref, tp_ref, came_ref, keep_ref, send_ref, all_ref, acc):
    add_slots(wanted_ref, tp_ref, came_ref, acc, keep_ref, send_ref)
    held, span, width = acc.shape[0] - 1, acc.shape[1], acc.shape[2]
    for i in range(held):
        all_ref[:, i * span : (i + 1) * span] = acc[1 + i].T.astype(BF16)


def key_totals_kernel(wanted_ref, tp_ref, came_ref, keep_ref, send_ref, part_ref, acc):
    add_slots(wanted_ref, tp_ref, came_ref, acc, keep_ref, send_ref)
    span = acc.shape[1]

    def step(i, carry):
        return carry + came_ref[i, span:].astype(F32)

    count, rows, width = part_ref.shape
    total = lax.fori_loop(0, count, step, jnp.zeros((rows, width), F32), unroll=8).astype(BF16)
    for i in range(count):
        part_ref[i] = total


def weight_kernel(store_ref, vt_ref, buf_ref, out_ref):
    part = dot(vt_ref[...], store_ref[...], 1, 0)
    part = part.T.astype(BF16)
    rows = out_ref.shape[1]
    for i in range(out_ref.shape[0]):
        out_ref[i] = part[i * rows : (i + 1) * rows]


def back_kernel(a0, a1, a2, a3, w0, w1, w2, w3, out_ref):
    a = jnp.concatenate([a0[...], a1[...], a2[...], a3[...]], axis=1)
    step = 256
    for n in range(0, out_ref.shape[1], step):
        w = jnp.concatenate([r[n : n + step] for r in (w0, w1, w2, w3)], axis=1)
        out_ref[:, n : n + step] = dot(a, w, 1, 1).astype(BF16)


def back(parts, weights, tile=256):
    rows, width = parts[0].shape
    depth = weights[0].shape[0]
    return pl.pallas_call(
        back_kernel,
        grid=(rows // tile,),
        out_shape=jax.ShapeDtypeStruct((rows, depth), BF16),
        in_specs=[pl.BlockSpec((tile, width), lambda i: (i, 0))] * 4
        + [pl.BlockSpec((depth, width), lambda i: (0, 0))] * 4,
        out_specs=pl.BlockSpec((tile, depth), lambda i: (i, 0)),
        name="back",
    )(*parts, *weights)


def body(hidden, passage_store, passage_ids, query_weight, gate_weight, key_weight, value_weight, output_grad):
    owners = lax.axis_size("st")
    held, span, depth = passage_store.shape
    blocks, per_block = passage_ids.shape
    width = query_weight.shape[1]
    tokens = hidden.shape[0]
    tp = lax.axis_index("tp").astype(jnp.int32).reshape(1)

    ids = passage_ids.reshape(-1)
    asked = (ids // held)[None, :] == jnp.arange(owners, dtype=jnp.int32)[:, None]
    request = jnp.sum(jnp.where(asked, (ids % held + 1)[None, :], 0), axis=1)
    wanted = exchange(jnp.broadcast_to(request[:, None], (owners, 128)))

    store_rows = passage_store.reshape(held * span, depth)
    keys = jnp.dot(store_rows, key_weight, preferred_element_type=F32).astype(BF16).reshape(held, span, width)
    came_keys = exchange(pick(wanted, keys))
    values = jnp.dot(store_rows, value_weight, preferred_element_type=F32).astype(BF16).reshape(held, span, width)
    came_values = exchange(pick(wanted, values))

    queries = jnp.dot(hidden, query_weight, preferred_element_type=F32).astype(BF16)
    gates = jnp.dot(hidden, gate_weight, preferred_element_type=F32)
    d_attended = (output_grad.astype(F32) * gates * jax.nn.sigmoid(gates)).astype(BF16)

    probs, back_values = pl.pallas_call(
        functools.partial(probs_kernel, held),
        out_shape=(
            jax.ShapeDtypeStruct((tokens, per_block * span), F32),
            jax.ShapeDtypeStruct((owners, span, width), BF16),
        ),
        in_specs=[SMEM, VMEM, VMEM, VMEM],
        out_specs=(VMEM, VMEM),
        name="probs",
    )(passage_ids, queries, d_attended, came_keys)
    came_dvalues = exchange(back_values)

    piece = depth // owners
    half_tokens = jax.ShapeDtypeStruct((2, tokens // 2, width), BF16)
    keep_tokens, send_tokens, back_keys = pl.pallas_call(
        functools.partial(grads_kernel, held),
        out_shape=(half_tokens, half_tokens, jax.ShapeDtypeStruct((owners, span + piece, width), BF16)),
        in_specs=[SMEM, SMEM] + [VMEM] * 7,
        out_specs=(VMEM, VMEM, VMEM),
        name="grads",
    )(passage_ids, tp, queries, d_attended, gates, output_grad, probs, came_keys, came_values)

    half_held = jax.ShapeDtypeStruct((held // 2, span, width), BF16)
    keep_values, send_values, values_across = pl.pallas_call(
        value_totals_kernel,
        out_shape=(half_held, half_held, jax.ShapeDtypeStruct((width, held * span), BF16)),
        in_specs=[SMEM, SMEM, VMEM],
        out_specs=(VMEM, VMEM, VMEM),
        scratch_shapes=[pltpu.VMEM((held + 1, span, width), F32)],
        name="value_totals",
    )(wanted, tp, came_dvalues)

    tile = 256
    back_keys = pl.pallas_call(
        weight_kernel,
        grid=(depth // tile,),
        out_shape=jax.ShapeDtypeStruct(back_keys.shape, BF16),
        in_specs=[
            pl.BlockSpec((held * span, tile), lambda i: (0, i)),
            pl.BlockSpec((width, held * span), lambda i: (0, 0)),
            pl.BlockSpec(memory_space=pl.ANY),
        ],
        out_specs=pl.BlockSpec((tile // piece, piece, width), lambda i: (i, span // piece, 0)),
        input_output_aliases={2: 0},
        name="weight",
    )(store_rows, values_across, back_keys)
    came_dkeys = exchange(back_keys)

    keep_keys, send_keys, summed = pl.pallas_call(
        key_totals_kernel,
        out_shape=(half_held, half_held, jax.ShapeDtypeStruct((owners, piece, width), BF16)),
        in_specs=[SMEM, SMEM, VMEM],
        out_specs=(VMEM, VMEM, VMEM),
        scratch_shapes=[pltpu.VMEM((held + 1, span, width), F32)],
        name="key_totals",
    )(wanted, tp, came_dkeys)
    grad_value_weight = exchange(summed).reshape(depth, width).astype(F32)

    other_query, other_gate, other_key, other_value = (
        swap_tp(w) for w in (query_weight, gate_weight, key_weight, value_weight)
    )
    other_tokens = swap_tp(send_tokens)
    other_values = swap_tp(send_values)
    other_keys = swap_tp(send_keys)
    grad_hidden = back(
        (keep_tokens[0], other_tokens[0], keep_tokens[1], other_tokens[1]),
        (query_weight, other_query, gate_weight, other_gate),
    )
    rows = held // 2 * span
    grad_store = back(
        tuple(t.reshape(rows, width) for t in (keep_keys, other_keys, keep_values, other_values)),
        (key_weight, other_key, value_weight, other_value),
    ).reshape(held // 2, span, depth)
    return grad_hidden, grad_store, grad_value_weight


def solution(mesh):
    placed = (
        P("st", None),
        P("st", None, None),
        P("st", None),
        P(None, "tp"),
        P(None, "tp"),
        P(None, "tp"),
        P(None, "tp"),
        P("st", "tp"),
    )
    return jax.shard_map(
        body,
        mesh=mesh,
        in_specs=placed,
        out_specs=(P(("st", "tp"), None), P(("st", "tp"), None, None), P(None, "tp")),
        check_vma=False,
    )
```

time: 347 us -> 229 us (0.66)
  waiting for transfers between devices: 159 us -> 106 us
  Pallas kernels: 0 us -> 49.3 us
  matrix products: 65.9 us -> 19.4 us
  local copies, waits for them, and re-layouts: 41.1 us -> 3.8 us
  between operations: 15.5 us -> 0.78 us
  blocking collectives: 13.1 us -> 0 us
  other arithmetic: 9.19 us -> 1.65 us
  starting transfers between devices: 41.3 us -> 47.1 us
    psum x1 -> x0, waiting for transfers between devices: 82.2 us -> none  [body(): grad_value_weight = lax.psum(weight_part, 'st')]
    pallas_call x0 -> x9, Pallas kernels: none -> 49.3 us  [the longest x2 13.5 us: back(): pl.pallas_call(back_kernel, grid=(rows // tile,), out_shape=jax.ShapeDtyp...]
    dot_general x17 -> x4, matrix products: 65.9 us -> 19.4 us  [the longest x1 6.93 us: body(): jnp.dot(store_rows, value_weight, preferred_element_type=F32).astype(BF16)]
    all_to_all x6, waiting for transfers between devices: 74.7 us -> 105 us  [exchange(): return lax.all_to_all(x, 'st', split_axis=0, concat_axis=0, tiled=True)]
    all_to_all x3 -> x0, blocking collectives: 13.1 us -> none  [the longest x1 4.58 us: body(): lax.all_to_all(value_low, 'tp', split_axis=0, concat_axis=2, tiled=True)]
    scatter x2 -> x0, local copies, waits for them, and re-layouts: 11.8 us -> none  [the longest x1 6.47 us: body(): jnp.zeros((slot_total, span_rows, local_width), jnp.float32).at[slot_flat]]
    gather x4 -> x0, local copies, waits for them, and re-layouts: 9.38 us -> none  [the longest x1 3.17 us: body(): came_keys.reshape(owner_count * capacity, span_rows, local_width)[slot_flat]]
    unnamed x23 -> x11, local copies, waits for them, and re-layouts: 9.75 us -> 1.53 us
  transfers between devices with their start and end apart: 11 -> 13, of which waited for: 6 -> 7; matrix products, arithmetic and copies ran while one was open for 33% -> 9% of each run, Pallas kernels for 0% -> 14%
where the time goes in v1:
time: 229 us; the launch traced here: 228 us
  waiting for transfers between devices  106 us (46%)
  Pallas kernels  49.3 us (22%)
  starting transfers between devices  47.1 us (21%)
  matrix products  19.4 us (8%)
  local copies, waits for them, and re-layouts  3.8 us (2%)
    all_to_all x6, waiting for transfers between devices, exchange(): return lax.all_to_all(x, 'st', split_axis=0, concat_axis=0, tiled=True)  105 us
    all_to_all x6, starting transfers between devices, exchange(): return lax.all_to_all(x, 'st', split_axis=0, concat_axis=0, tiled=True)  45.3 us
    pallas_call x2, Pallas kernels, back(): pl.pallas_call(back_kernel, grid=(rows // tile,), out_shape=jax.ShapeDtyp...  13.5 us
    pallas_call x1, Pallas kernels, body(): pl.pallas_call(weight_kernel, grid=(depth // tile,), out_shape=jax.ShapeD...  8.94 us
    pallas_call x1, Pallas kernels, body(): pl.pallas_call(functools.partial(grads_kernel, held), out_shape=(half_tok...  7.12 us
    dot_general x1, matrix products, body(): jnp.dot(store_rows, value_weight, preferred_element_type=F32).astype(BF16)  6.93 us
    dot_general x1, matrix products, body(): jnp.dot(store_rows, key_weight, preferred_element_type=F32).astype(BF16)  6.93 us
    pallas_call x2, Pallas kernels, pick(): pl.pallas_call(pick_kernel, out_shape=jax.ShapeDtypeStruct((wanted.shape[...  5.5 us
  transfers between devices with their start and end apart: 13, of which 7 were waited for; matrix products, arithmetic and copies ran while one was open for 9% of the time, Pallas kernels for 14%

profile of v1, /device:TPU:0, one launch (start us, length us, event | category | flops | bytes accessed | tf_op | source)
XLA Modules:
  0.0 228.2 jit_solution(12191847153082773404)
XLA Ops:
  0.6 0.0 copy-start
  0.6 0.9 copy.23.ids_ref
  1.6 0.0 copy-start.4
  1.6 0.1 reshape.96
  1.6 0.1 select_reduce_fusion
  1.7 0.8 broadcast_in_dim.23
  2.5 11.5 %all-to-all-start = ((s32[64,1,128]{2,1,0:T(1,128)}), s32[64,1,128]{2,1,0:T(1,128)S(1)}, u32[]{:S(2)}, u32[]{:S(2)}) async-start(s32[64,1,128]{2,1,0:T(1,128)} %broadcast_in_dim.23), calls=%async_computation | async-start | bytes 65536 | tf_op jit(solution)/shard_map/all_to_all | solution.py:26
  14.0 6.9 %convolution_convert_fusion.1 = bf16[2048,256]{1,0:T(8,128)(2,1)} fusion(bf16[2048,2048]{1,0:T(8,128)(2,1)} %bitcast.29, bf16[2048,256]{1,0:T(8,128)(2,1)} %w0.3), kind=kOutput, calls=%fused_computation.1 | convolution fusion | flops 2148007936 | bytes 10485760 | tf_op jit(solution)/shard_map/dot_general | solution.py:176
  21.0 0.0 copy-done.4
  21.0 2.6 %all-to-all-done = s32[64,1,128]{2,1,0:T(1,128)S(1)} async-done(((s32[64,1,128]{2,1,0:T(1,128)}), s32[64,1,128]{2,1,0:T(1,128)S(1)}, u32[]{:S(2)}, u32[]{:S(2)}) %all-to-all-start) | async-done | bytes 32800 | tf_op jit(solution)/shard_map/all_to_all | solution.py:26
  23.5 0.0 copy-start.1
  23.5 0.6 copy-done.1
  24.1 2.7 %pick.2 = bf16[64,64,256]{2,1,0:T(8,128)(2,1)} custom-call(s32[64,128]{1,0:T(8,128)} %bitcast.35, bf16[32,64,256]{2,1,0:T(8,128)(2,1)} %bitcast.33), custom_call_target="tpu_custom_call" | custom-call | tf_op jit(solution)/shard_map/pick/pallas_call | solution.py:38
  26.9 8.0 %all-to-all-start.1 = ((bf16[64,64,256]{2,1,0:T(8,128)(2,1)}), bf16[64,64,256]{2,1,0:T(8,128)(2,1)}, u32[]{:S(2)}, u32[]{:S(2)}) async-start(bf16[64,64,256]{2,1,0:T(8,128)(2,1)} %pick.2), calls=%async_computation.1 | async-start | bytes 4194304 | tf_op jit(solution)/shard_map/all_to_all | solution.py:26
  34.9 6.9 %convolution_convert_fusion = bf16[2048,256]{1,0:T(8,128)(2,1)} fusion(bf16[2048,2048]{1,0:T(8,128)(2,1)} %bitcast.30, bf16[2048,256]{1,0:T(8,128)(2,1)} %w2.3), kind=kOutput, calls=%fused_computation | convolution fusion | flops 2148007936 | bytes 10485760 | tf_op jit(solution)/shard_map/dot_general | solution.py:178
  41.9 2.7 %pick.3 = bf16[64,64,256]{2,1,0:T(8,128)(2,1)} custom-call(s32[64,128]{1,0:T(8,128)} %bitcast.36, bf16[32,64,256]{2,1,0:T(8,128)(2,1)} %bitcast.34), custom_call_target="tpu_custom_call" | custom-call | tf_op jit(solution)/shard_map/pick/pallas_call | solution.py:38
  44.6 19.6 %all-to-all-done.1.k_ref = bf16[64,64,256]{2,1,0:T(8,128)(2,1)} async-done(((bf16[64,64,256]{2,1,0:T(8,128)(2,1)}), bf16[64,64,256]{2,1,0:T(8,128)(2,1)}, u32[]{:S(2)}, u32[]{:S(2)}) %all-to-all-start.1) | async-done | bytes 2097184 | tf_op jit(solution)/shard_map/all_to_all | solution.py:26
  64.2 6.0 %all-to-all-start.2 = ((bf16[64,64,256]{2,1,0:T(8,128)(2,1)}), bf16[64,64,256]{2,1,0:T(8,128)(2,1)}, u32[]{:S(2)}, u32[]{:S(2)}) async-start(bf16[64,64,256]{2,1,0:T(8,128)(2,1)} %pick.3), calls=%async_computation.2 | async-start | bytes 4194304 | tf_op jit(solution)/shard_map/all_to_all | solution.py:26
  70.2 0.0 copy-done
  70.2 0.0 copy-start.2
  70.2 2.7 %convolution_convert_fusion.2.q_ref = bf16[512,256]{1,0:T(8,128)(2,1)} fusion(bf16[512,2048]{1,0:T(8,128)(2,1)S(1)} %copy-done, bf16[2048,256]{1,0:T(8,128)(2,1)} %w0.2), kind=kOutput, calls=%fused_computation.2 | convolution fusion | flops 537001984 | bytes 3407872 | tf_op jit(solution)/shard_map/dot_general | solution.py:181
  72.9 0.0 copy-done.2
  72.9 2.8 %multiply_convert_fusion = (bf16[512,256]{1,0:T(8,128)(2,1)}, f32[512,256]{1,0:T(8,128)}) fusion(bf16[512,256]{1,0:T(8,128)(2,1)S(1)} %copy-done.2, bf16[512,2048]{1,0:T(8,128)(2,1)S(1)} %copy-done, bf16[2048,256]{1,0:T(8,128)(2,1)} %w2.2), kind=kOutput, calls=%fused_computation.4 | convolution fusion | flops 537788416 | bytes 4194304 | tf_op jit(solution)/shard_map/dot_general | solution.py:182
  75.7 5.4 %probs.1 = (f32[512,256]{1,0:T(8,128)}, bf16[64,64,256]{2,1,0:T(8,128)(2,1)}) custom-call(s32[8,4]{1,0:T(8,128)} %copy-done.4, bf16[512,256]{1,0:T(8,128)(2,1)} %convolution_convert_fusion.2.q_ref, bf16[512,256]{1,0:T(8,128)(2,1)} %get-tuple-element.31.da_ref, bf16[64,64,256]{2,1,0:T(8,128)(2,1)} %all-to-all-done.1.k_ref), custom_call_target="tpu_custom_call" | custom-call | tf_op jit(solution)/shard_map/probs/pallas_call | solution.py:185
  81.1 18.6 %all-to-all-done.2.v_ref = bf16[64,64,256]{2,1,0:T(8,128)(2,1)} async-done(((bf16[64,64,256]{2,1,0:T(8,128)(2,1)}), bf16[64,64,256]{2,1,0:T(8,128)(2,1)}, u32[]{:S(2)}, u32[]{:S(2)}) %all-to-all-start.2) | async-done | bytes 2097184 | tf_op jit(solution)/shard_map/all_to_all | solution.py:26
  99.7 6.3 %all-to-all-start.3 = ((bf16[64,64,256]{2,1,0:T(8,128)(2,1)}), bf16[64,64,256]{2,1,0:T(8,128)(2,1)}, u32[]{:S(2)}, u32[]{:S(2)}) async-start(bf16[64,64,256]{2,1,0:T(8,128)(2,1)} %get-tuple-element.17), calls=%async_computation.3 | async-start | bytes 4194304 | tf_op jit(solution)/shard_map/all_to_all | solution.py:26
  106.0 7.1 %grads.1 = (bf16[2,256,256]{2,1,0:T(8,128)(2,1)}, bf16[2,256,256]{2,1,0:T(8,128)(2,1)}, bf16[64,96,256]{2,1,0:T(8,128)(2,1)}) custom-call(s32[8,4]{1,0:T(8,128)} %copy-done.4, s32[1]{0:T(128)} %bitcast.tp_ref, bf16[512,256]{1,0:T(8,128)(2,1)} %convolution_convert_fusion.2.q_ref, bf16[512,256]{1,0:T(8,128)(2,1)} %get-tuple-element.31.da_ref, ...), custom_call_target="tpu_custom_call" | custom-call | tf_op jit(solution)/shard_map/grads/pallas_call | solution.py:199
  113.1 22.2 %all-to-all-done.3.came_ref = bf16[64,64,256]{2,1,0:T(8,128)(2,1)} async-done(((bf16[64,64,256]{2,1,0:T(8,128)(2,1)}), bf16[64,64,256]{2,1,0:T(8,128)(2,1)}, u32[]{:S(2)}, u32[]{:S(2)}) %all-to-all-start.3) | async-done | bytes 2097184 | tf_op jit(solution)/shard_map/all_to_all | solution.py:26
  135.4 4.7 %value_totals.1 = (bf16[16,64,256]{2,1,0:T(8,128)(2,1)}, bf16[16,64,256]{2,1,0:T(8,128)(2,1)}, bf16[256,2048]{1,0:T(8,128)(2,1)}) custom-call(s32[64,128]{1,0:T(8,128)} %bitcast.37, s32[1]{0:T(128)} %bitcast.tp_ref, bf16[64,64,256]{2,1,0:T(8,128)(2,1)} %all-to-all-done.3.came_ref), custom_call_target="tpu_custom_call" | custom-call | tf_op jit(solution)/shard_map/value_totals/pallas_call | solution.py:208
  140.1 8.9 %weight.1 = bf16[64,96,256]{2,1,0:T(8,128)(2,1)} custom-call(bf16[2048,2048]{1,0:T(8,128)(2,1)} %bitcast.31, bf16[256,2048]{1,0:T(8,128)(2,1)} %get-tuple-element.18.vt_ref, bf16[64,96,256]{2,1,0:T(8,128)(2,1)} %get-tuple-element.19.buf_ref), custom_call_target="tpu_custom_call", output_to_operand_aliasing={{}: (2, {})} | custom-call | tf_op jit(solution)/shard_map/weight/pallas_call | solution.py:218
  149.0 6.1 %all-to-all-start.4 = ((bf16[64,96,256]{2,1,0:T(8,128)(2,1)}), bf16[64,96,256]{2,1,0:T(8,128)(2,1)}, u32[]{:S(2)}, u32[]{:S(2)}) async-start(bf16[64,96,256]{2,1,0:T(8,128)(2,1)} %weight.1), calls=%async_computation.4 | async-start | bytes 6291456 | tf_op jit(solution)/shard_map/all_to_all | solution.py:26
  155.1 0.0 copy-start.3
  155.1 0.1 collective-permute-start.1
  155.2 0.5 collective-permute-start.2
  155.7 0.1 collective-permute-start.5
  155.8 0.4 collective-permute-start.6
  156.2 40.2 %all-to-all-done.4.came_ref = bf16[64,96,256]{2,1,0:T(8,128)(2,1)} async-done(((bf16[64,96,256]{2,1,0:T(8,128)(2,1)}), bf16[64,96,256]{2,1,0:T(8,128)(2,1)}, u32[]{:S(2)}, u32[]{:S(2)}) %all-to-all-start.4) | async-done | bytes 3145760 | tf_op jit(solution)/shard_map/all_to_all | solution.py:26
  196.5 4.1 %key_totals.1 = (bf16[16,64,256]{2,1,0:T(8,128)(2,1)}, bf16[16,64,256]{2,1,0:T(8,128)(2,1)}, bf16[64,32,256]{2,1,0:T(8,128)(2,1)}) custom-call(s32[64,128]{1,0:T(8,128)} %bitcast.38, s32[1]{0:T(128)} %bitcast.tp_ref, bf16[64,96,256]{2,1,0:T(8,128)(2,1)} %all-to-all-done.4.came_ref), custom_call_target="tpu_custom_call" | custom-call | tf_op jit(solution)/shard_map/key_totals/pallas_call | solution.py:233
  200.6 7.3 %all-to-all-start.5 = ((bf16[64,32,256]{2,1,0:T(8,128)(2,1)}), bf16[64,32,256]{2,1,0:T(8,128)(2,1)S(1)}, u32[]{:S(2)}, u32[]{:S(2)}) async-start(bf16[64,32,256]{2,1,0:T(8,128)(2,1)} %get-tuple-element.24), calls=%async_computation.5 | async-start | bytes 2097152 | tf_op jit(solution)/shard_map/all_to_all | solution.py:26
  207.9 0.1 collective-permute-start
  208.0 0.0 collective-permute-done.1.w1
  208.0 0.5 collective-permute-start.4
  208.5 1.2 collective-permute-done
  209.7 0.1 collective-permute-start.3
  209.9 0.0 copy-done.3
  209.9 0.7 slice_bitcast_fusion.2
  210.6 0.7 slice_bitcast_fusion
  211.3 0.0 collective-permute-done.2.w3
  211.3 4.6 %back.2 = bf16[256,2048]{1,0:T(8,128)(2,1)} custom-call(bf16[256,256]{1,0:T(8,128)(2,1)} %get-tuple-element.28.a0, bf16[256,256]{1,0:T(8,128)(2,1)} %get-tuple-element.26.a1, bf16[256,256]{1,0:T(8,128)(2,1)} %get-tuple-element.27.a2, bf16[256,256]{1,0:T(8,128)(2,1)} %get-tuple-element.25.a3, bf16[2048,256]{1,0:T(8,128)(2,1)} %w0.2, ...), custom_call_target="tpu_custom_call" | custom-call | tf_op jit(solution)/shard_map/back/pallas_call | solution.py:151
  216.0 0.0 collective-permute-done.5.w1
  216.0 0.0 collective-permute-done.6.w3
  216.0 0.0 collective-permute-done.4
  216.0 0.0 collective-permute-done.3
  216.0 8.9 %back.3 = bf16[1024,2048]{1,0:T(8,128)(2,1)} custom-call(bf16[1024,256]{1,0:T(8,128)(2,1)} %bitcast.40, bf16[1024,256]{1,0:T(8,128)(2,1)} %bitcast.10.a1, bf16[1024,256]{1,0:T(8,128)(2,1)} %bitcast.39, bf16[1024,256]{1,0:T(8,128)(2,1)} %bitcast.12.a3, bf16[2048,256]{1,0:T(8,128)(2,1)} %w0.3, bf16[2048,256]{1,0:T(8,128)(2,1)} %collective-permute-done.5.w1, ...), custom_call_target="tpu_custom_call" | custom-call | tf_op jit(solution)/shard_map/back/pallas_call | solution.py:151
  224.9 1.8 all-to-all-done.5
  226.7 1.5 bitcast_convert_fusion
  (1 shorter events, 0.0 us)
Async XLA Ops:
  0.6 69.5 %copy-start = (bf16[512,2048]{1,0:T(8,128)(2,1)S(1)}, bf16[512,2048]{1,0:T(8,128)(2,1)}, u32[]{:S(2)}) copy-start(bf16[512,2048]{1,0:T(8,128)(2,1)} %param.8) | copy-start | bytes 6291460
  1.6 19.4 %copy-start.4 = (s32[8,4]{1,0:T(8,128)}, s32[8,4]{1,0:T(8,128)S(1)}, u32[]{:S(2)}) copy-start(s32[8,4]{1,0:T(8,128)S(1)} %copy.23.ids_ref) | copy-start | bytes 388
  2.5 21.0 %all-to-all-start = ((s32[64,1,128]{2,1,0:T(1,128)}), s32[64,1,128]{2,1,0:T(1,128)S(1)}, u32[]{:S(2)}, u32[]{:S(2)}) async-start(s32[64,1,128]{2,1,0:T(1,128)} %broadcast_in_dim.23), calls=%async_computation | async-start | bytes 65536 | tf_op jit(solution)/shard_map/all_to_all | solution.py:26
  23.5 0.6 copy-start.1
  26.9 37.3 %all-to-all-start.1 = ((bf16[64,64,256]{2,1,0:T(8,128)(2,1)}), bf16[64,64,256]{2,1,0:T(8,128)(2,1)}, u32[]{:S(2)}, u32[]{:S(2)}) async-start(bf16[64,64,256]{2,1,0:T(8,128)(2,1)} %pick.2), calls=%async_computation.1 | async-start | bytes 4194304 | tf_op jit(solution)/shard_map/all_to_all | solution.py:26
  64.2 35.5 %all-to-all-start.2 = ((bf16[64,64,256]{2,1,0:T(8,128)(2,1)}), bf16[64,64,256]{2,1,0:T(8,128)(2,1)}, u32[]{:S(2)}, u32[]{:S(2)}) async-start(bf16[64,64,256]{2,1,0:T(8,128)(2,1)} %pick.3), calls=%async_computation.2 | async-start | bytes 4194304 | tf_op jit(solution)/shard_map/all_to_all | solution.py:26
  70.2 2.7 %copy-start.2 = (bf16[512,256]{1,0:T(8,128)(2,1)S(1)}, bf16[512,256]{1,0:T(8,128)(2,1)}, u32[]{:S(2)}) copy-start(bf16[512,256]{1,0:T(8,128)(2,1)} %og_ref.1) | copy-start | bytes 786436
  99.7 35.7 %all-to-all-start.3 = ((bf16[64,64,256]{2,1,0:T(8,128)(2,1)}), bf16[64,64,256]{2,1,0:T(8,128)(2,1)}, u32[]{:S(2)}, u32[]{:S(2)}) async-start(bf16[64,64,256]{2,1,0:T(8,128)(2,1)} %get-tuple-element.17), calls=%async_computation.3 | async-start | bytes 4194304 | tf_op jit(solution)/shard_map/all_to_all | solution.py:26
  149.0 47.5 %all-to-all-start.4 = ((bf16[64,96,256]{2,1,0:T(8,128)(2,1)}), bf16[64,96,256]{2,1,0:T(8,128)(2,1)}, u32[]{:S(2)}, u32[]{:S(2)}) async-start(bf16[64,96,256]{2,1,0:T(8,128)(2,1)} %weight.1), calls=%async_computation.4 | async-start | bytes 6291456 | tf_op jit(solution)/shard_map/all_to_all | solution.py:26
  155.1 54.8 %copy-start.3 = (bf16[2,256,256]{2,1,0:T(8,128)(2,1)S(1)}, bf16[2,256,256]{2,1,0:T(8,128)(2,1)}, u32[]{:S(2)}) copy-start(bf16[2,256,256]{2,1,0:T(8,128)(2,1)} %get-tuple-element.15) | copy-start | bytes 786436
  155.1 52.9 %collective-permute-start.1 = (bf16[2048,256]{1,0:T(8,128)(2,1)}, bf16[2048,256]{1,0:T(8,128)(2,1)}, u32[]{:S(2)}, u32[]{:S(2)}) collective-permute-start(bf16[2048,256]{1,0:T(8,128)(2,1)} %w0.2), channel_id=1, source_target_pairs={{0,1},{1,0},{2,3},{3,2},{4,5},{5,4},{6,7},{7,6},{8,9},{9,8},{10,11... | collective-permute-start | bytes 3145736 | tf_op jit(solution)/shard_map/ppermute | solution.py:22
  155.2 56.1 %collective-permute-start.2 = (bf16[2048,256]{1,0:T(8,128)(2,1)}, bf16[2048,256]{1,0:T(8,128)(2,1)}, u32[]{:S(2)}, u32[]{:S(2)}) collective-permute-start(bf16[2048,256]{1,0:T(8,128)(2,1)} %w2.2), channel_id=1, source_target_pairs={{0,1},{1,0},{2,3},{3,2},{4,5},{5,4},{6,7},{7,6},{8,9},{9,8},{10,11... | collective-permute-start | bytes 3145736 | tf_op jit(solution)/shard_map/ppermute | solution.py:22
  155.7 60.3 %collective-permute-start.5 = (bf16[2048,256]{1,0:T(8,128)(2,1)}, bf16[2048,256]{1,0:T(8,128)(2,1)}, u32[]{:S(2)}, u32[]{:S(2)}) collective-permute-start(bf16[2048,256]{1,0:T(8,128)(2,1)} %w0.3), channel_id=1, source_target_pairs={{0,1},{1,0},{2,3},{3,2},{4,5},{5,4},{6,7},{7,6},{8,9},{9,8},{10,11... | collective-permute-start | bytes 3145736 | tf_op jit(solution)/shard_map/ppermute | solution.py:22
  155.8 60.2 %collective-permute-start.6 = (bf16[2048,256]{1,0:T(8,128)(2,1)}, bf16[2048,256]{1,0:T(8,128)(2,1)}, u32[]{:S(2)}, u32[]{:S(2)}) collective-permute-start(bf16[2048,256]{1,0:T(8,128)(2,1)} %w2.3), channel_id=1, source_target_pairs={{0,1},{1,0},{2,3},{3,2},{4,5},{5,4},{6,7},{7,6},{8,9},{9,8},{10,11... | collective-permute-start | bytes 3145736 | tf_op jit(solution)/shard_map/ppermute | solution.py:22
  200.6 26.1 %all-to-all-start.5 = ((bf16[64,32,256]{2,1,0:T(8,128)(2,1)}), bf16[64,32,256]{2,1,0:T(8,128)(2,1)S(1)}, u32[]{:S(2)}, u32[]{:S(2)}) async-start(bf16[64,32,256]{2,1,0:T(8,128)(2,1)} %get-tuple-element.24), calls=%async_computation.5 | async-start | bytes 2097152 | tf_op jit(solution)/shard_map/all_to_all | solution.py:26
  207.9 1.8 collective-permute-start
  208.0 8.0 %collective-permute-start.4 = (bf16[16,64,256]{2,1,0:T(8,128)(2,1)}, bf16[16,64,256]{2,1,0:T(8,128)(2,1)}, u32[]{:S(2)}, u32[]{:S(2)}) collective-permute-start(bf16[16,64,256]{2,1,0:T(8,128)(2,1)} %get-tuple-element.23), channel_id=1, source_target_pairs={{0,1},{1,0},{2,3},{3,2},{4,5},{5,4},{6,7},{7,6},{8,9},{9,8},{10,11... | collective-permute-start | bytes 1572872 | tf_op jit(solution)/shard_map/ppermute | solution.py:22
  209.7 6.2 %collective-permute-start.3 = (bf16[16,64,256]{2,1,0:T(8,128)(2,1)}, bf16[16,64,256]{2,1,0:T(8,128)(2,1)}, u32[]{:S(2)}, u32[]{:S(2)}) collective-permute-start(bf16[16,64,256]{2,1,0:T(8,128)(2,1)} %get-tuple-element.21), channel_id=1, source_target_pairs={{0,1},{1,0},{2,3},{3,2},{4,5},{5,4},{6,7},{7,6},{8,9},{9,8},{10,11... | collective-permute-start | bytes 1572872 | tf_op jit(solution)/shard_map/ppermute | solution.py:22

commit v2 on v1

v2 whole, which is shorter than its diff:
```python
import functools

import jax
import jax.numpy as jnp
from jax import lax
from jax.experimental import pallas as pl
from jax.experimental.pallas import tpu as pltpu
from jax.sharding import PartitionSpec as P

HEAD_DIM = 256
PAUSE = 2850
F32 = jnp.float32
BF16 = jnp.bfloat16
VMEM = pl.BlockSpec(memory_space=pltpu.VMEM)
SMEM = pl.BlockSpec(memory_space=pltpu.SMEM)
ANY = pl.BlockSpec(memory_space=pl.ANY)


def dot(a, b, ca, cb):
    return lax.dot_general(a, b, (((ca,), (cb,)), ((), ())), preferred_element_type=F32)


def swap_tp(x):
    return lax.ppermute(x, "tp", [(0, 1), (1, 0)])


def exchange(x):
    return lax.all_to_all(x, "st", split_axis=0, concat_axis=0, tiled=True)


def request_kernel(held, ids_ref, out_ref):
    per, blocks = ids_ref.shape
    out_ref[...] = jnp.zeros_like(out_ref)
    for b in range(blocks):
        for j in range(per):
            at = ids_ref[j, b]
            owner = lax.div(at, held)
            out_ref[pl.ds(owner, 1)] = jnp.full((1, out_ref.shape[1]), at - owner * held + 1, jnp.int32)


def pick_kernel(wanted_ref, pause_ref, rows_ref, *refs):
    out_ref, wait, sem = refs[-3:]
    if pause_ref is not None:
        wait[...] = lax.fori_loop(0, pause_ref[0], lambda i, c: jnp.tanh(c), jnp.zeros(wait.shape, F32))

    def step(i, carry):
        at = jnp.maximum(wanted_ref[i, 0] - 1, 0)
        pltpu.make_async_copy(rows_ref.at[at], out_ref.at[i], sem).start()
        return carry

    lax.fori_loop(0, out_ref.shape[0], step, 0, unroll=8)
    pltpu.make_async_copy(out_ref, out_ref, sem).wait()


def pick(wanted, pause, rows, *after):
    return pl.pallas_call(
        pick_kernel,
        out_shape=jax.ShapeDtypeStruct((wanted.shape[0], *rows.shape[1:]), rows.dtype),
        in_specs=[SMEM, SMEM, VMEM] + [ANY] * len(after),
        out_specs=ANY,
        scratch_shapes=[pltpu.VMEM((8, 128), F32), pltpu.SemaphoreType.DMA],
        name="pick",
    )(wanted, pause, rows, *after)


def probs_kernel(held, ids_ref, q_ref, da_ref, k_ref, p_ref, dv_ref):
    per, blocks = ids_ref.shape
    rows = q_ref.shape[0] // blocks
    span = k_ref.shape[1]
    scale = HEAD_DIM**-0.5
    for b in range(blocks):
        mine = slice(b * rows, (b + 1) * rows)
        owner = [lax.div(ids_ref[j, b], held) for j in range(per)]
        k = jnp.concatenate([k_ref[o] for o in owner], axis=0)
        s = dot(q_ref[mine], k, 1, 1) * scale
        e = jnp.exp(s - jnp.max(s, axis=1, keepdims=True))
        p = e / jnp.sum(e, axis=1, keepdims=True)
        p_ref[mine] = p
        dv = dot(p.astype(BF16), da_ref[mine], 0, 0).astype(BF16)
        for j in range(per):
            dv_ref[owner[j]] = dv[j * span : (j + 1) * span]


def grads_kernel(held, ids_ref, tp_ref, q_ref, da_ref, g_ref, og_ref, p_ref, k_ref, v_ref, keep_dq, keep_dg, send_dq, send_dg, dk_ref):
    per, blocks = ids_ref.shape
    rows = q_ref.shape[0] // blocks
    span = k_ref.shape[1]
    scale = HEAD_DIM**-0.5
    half = blocks // 2
    for n in range(blocks):
        b = lax.rem(n + half * tp_ref[0], blocks)
        mine = pl.ds(pl.multiple_of(b * rows, rows), rows)
        owner = [lax.div(ids_ref[j, b], held) for j in range(per)]
        k = jnp.concatenate([k_ref[o] for o in owner], axis=0)
        v = jnp.concatenate([v_ref[o] for o in owner], axis=0)
        p = p_ref[mine]
        q = q_ref[mine]
        g = g_ref[mine]
        dp = dot(da_ref[mine], v, 1, 1)
        attended = dot(p.astype(BF16), v, 1, 0)
        centre = jnp.sum(p * dp, axis=1, keepdims=True)
        ds = (p * (dp - centre) * scale).astype(BF16)
        dq = dot(ds, k, 1, 0).astype(BF16)
        dk = dot(ds, q, 0, 0).astype(BF16)
        sg = jax.nn.sigmoid(g)
        dg = (og_ref[mine].astype(F32) * attended * sg * (1.0 + g * (1.0 - sg))).astype(BF16)
        for j in range(per):
            dk_ref[owner[j]] = dk[j * span : (j + 1) * span]
        at = slice((n % half) * rows, (n % half + 1) * rows)
        (keep_dq if n < half else send_dq)[at] = dq
        (keep_dg if n < half else send_dg)[at] = dg


def add_slots(wanted_ref, tp_ref, came_ref, acc, keep_ref, send_ref):
    acc[...] = jnp.zeros_like(acc)

    def step(i, carry):
        at = wanted_ref[i, 0]
        acc[at] = acc[at] + came_ref[i].astype(F32)
        return carry

    lax.fori_loop(0, came_ref.shape[0], step, 0, unroll=8)
    half = keep_ref.shape[0]
    tp = tp_ref[0]
    keep_ref[...] = acc[pl.ds(1 + half * tp, half)].astype(BF16)
    send_ref[...] = acc[pl.ds(1 + half * (1 - tp), half)].astype(BF16)


def add_slots_kernel(wanted_ref, tp_ref, came_ref, keep_ref, send_ref, acc):
    add_slots(wanted_ref, tp_ref, came_ref, acc, keep_ref, send_ref)


def value_totals_kernel(wanted_ref, tp_ref, came_ref, keep_ref, send_ref, all_ref, acc):
    add_slots(wanted_ref, tp_ref, came_ref, acc, keep_ref, send_ref)
    held, span = acc.shape[0] - 1, acc.shape[1]
    for i in range(held):
        all_ref[:, i * span : (i + 1) * span] = acc[1 + i].T.astype(BF16)


def weight_kernel(store_ref, vt_ref, out_ref):
    part = dot(vt_ref[...], store_ref[...], 1, 0).T.astype(BF16)
    rows = out_ref.shape[1]
    for i in range(out_ref.shape[0]):
        out_ref[i] = part[i * rows : (i + 1) * rows]


def back_kernel(terms, *refs):
    out_ref = refs[-1]
    a = jnp.concatenate([r[...] for r in refs[:terms]], axis=1)
    step = 256
    for n in range(0, out_ref.shape[1], step):
        w = jnp.concatenate([r[n : n + step] for r in refs[terms:-1]], axis=1)
        out_ref[:, n : n + step] = dot(a, w, 1, 1).astype(out_ref.dtype)


def back(terms, weights, dtype, tile=256):
    rows, width = terms[0].shape
    depth = weights[0].shape[0]
    return pl.pallas_call(
        functools.partial(back_kernel, len(terms)),
        grid=(rows // tile,),
        out_shape=jax.ShapeDtypeStruct((rows, depth), dtype),
        in_specs=[pl.BlockSpec((tile, width), lambda i: (i, 0))] * len(terms)
        + [pl.BlockSpec((depth, width), lambda i: (0, 0))] * len(weights),
        out_specs=pl.BlockSpec((tile, depth), lambda i: (i, 0)),
        name="back",
    )(*terms, *weights)


def body(hidden, passage_store, passage_ids, query_weight, gate_weight, key_weight, value_weight, output_grad):
    owners = lax.axis_size("st")
    held, span, depth = passage_store.shape
    _, per_block = passage_ids.shape
    width = query_weight.shape[1]
    tokens = hidden.shape[0]
    tp = lax.axis_index("tp").astype(jnp.int32).reshape(1)

    ids = passage_ids.T
    request = pl.pallas_call(
        functools.partial(request_kernel, held),
        out_shape=jax.ShapeDtypeStruct((owners, 128), jnp.int32),
        in_specs=[SMEM],
        out_specs=VMEM,
        name="request",
    )(ids)
    wanted = exchange(request)

    other_key, other_value = swap_tp(key_weight), swap_tp(value_weight)
    store_rows = passage_store.reshape(held * span, depth)
    keys = jnp.dot(store_rows, key_weight, preferred_element_type=F32).astype(BF16).reshape(held, span, width)
    pause = tp * PAUSE
    came_keys = exchange(pick(wanted, pause, keys, other_key, other_value))
    values = jnp.dot(store_rows, value_weight, preferred_element_type=F32).astype(BF16).reshape(held, span, width)
    came_values = exchange(pick(wanted, jnp.zeros_like(tp), values))

    queries = jnp.dot(hidden, query_weight, preferred_element_type=F32).astype(BF16)
    gates = jnp.dot(hidden, gate_weight, preferred_element_type=F32)
    d_attended = (output_grad.astype(F32) * gates * jax.nn.sigmoid(gates)).astype(BF16)

    probs, back_values = pl.pallas_call(
        functools.partial(probs_kernel, held),
        out_shape=(
            jax.ShapeDtypeStruct((tokens, per_block * span), F32),
            jax.ShapeDtypeStruct((owners, span, width), BF16),
        ),
        in_specs=[SMEM, VMEM, VMEM, VMEM],
        out_specs=(VMEM, VMEM),
        name="probs",
    )(ids, queries, d_attended, came_keys)
    came_dvalues = exchange(back_values)

    piece = depth // owners
    half_tokens = jax.ShapeDtypeStruct((tokens // 2, width), BF16)
    keep_dq, keep_dg, send_dq, send_dg, back_keys = pl.pallas_call(
        functools.partial(grads_kernel, held),
        out_shape=(half_tokens,) * 4 + (jax.ShapeDtypeStruct((owners, span, width), BF16),),
        in_specs=[SMEM, SMEM] + [VMEM] * 7,
        out_specs=(VMEM,) * 5,
        name="grads",
    )(ids, tp, queries, d_attended, gates, output_grad, probs, came_keys, came_values)

    half_held = jax.ShapeDtypeStruct((held // 2, span, width), BF16)
    keep_values, send_values, values_across = pl.pallas_call(
        value_totals_kernel,
        out_shape=(half_held, half_held, jax.ShapeDtypeStruct((width, held * span), BF16)),
        in_specs=[SMEM, SMEM, VMEM],
        out_specs=(VMEM, VMEM, VMEM),
        scratch_shapes=[pltpu.VMEM((held + 1, span, width), F32)],
        name="value_totals",
    )(wanted, tp, came_dvalues)

    came_dkeys = exchange(back_keys)
    tile = 256
    parts = pl.pallas_call(
        weight_kernel,
        grid=(depth // tile,),
        out_shape=jax.ShapeDtypeStruct((owners, piece, width), BF16),
        in_specs=[
            pl.BlockSpec((held * span, tile), lambda i: (0, i)),
            pl.BlockSpec((width, held * span), lambda i: (0, 0)),
        ],
        out_specs=pl.BlockSpec((tile // piece, piece, width), lambda i: (i, 0, 0)),
        name="weight",
    )(store_rows, values_across)
    came_parts = exchange(lax.optimization_barrier((parts, came_dkeys))[0])

    keep_keys, send_keys = pl.pallas_call(
        add_slots_kernel,
        out_shape=(half_held, half_held),
        in_specs=[SMEM, SMEM, VMEM],
        out_specs=(VMEM, VMEM),
        scratch_shapes=[pltpu.VMEM((held + 1, span, width), F32)],
        name="key_totals",
    )(wanted, tp, came_dkeys)
    keep_hidden = back((keep_dq, keep_dg), (query_weight, gate_weight), F32)
    send_hidden = back((send_dq, send_dg), (query_weight, gate_weight), BF16)
    rows = held // 2 * span
    keep_keys, send_keys, keep_values, send_values = (
        t.reshape(rows, width) for t in (keep_keys, send_keys, keep_values, send_values)
    )
    came_parts, keep_keys, send_keys, keep_hidden, send_hidden = lax.optimization_barrier(
        (came_parts, keep_keys, send_keys, keep_hidden, send_hidden)
    )
    summed = jnp.sum(came_parts.astype(F32), axis=0).astype(BF16)
    gathered = exchange(jnp.broadcast_to(summed, came_parts.shape))

    other_values = swap_tp(send_values)
    other_keys = swap_tp(send_keys)
    other_hidden = swap_tp(send_hidden)
    grad_hidden = (keep_hidden + other_hidden.astype(F32)).astype(BF16)
    grad_store = back(
        (keep_keys, other_keys, keep_values, other_values), (key_weight, other_key, value_weight, other_value), BF16
    ).reshape(held // 2, span, depth)
    gathered, grad_hidden, grad_store = lax.optimization_barrier((gathered, grad_hidden, grad_store))
    grad_value_weight = gathered.reshape(depth, width).astype(F32)
    return grad_hidden, grad_store, grad_value_weight


def solution(mesh):
    placed = (
        P("st", None),
        P("st", None, None),
        P("st", None),
        P(None, "tp"),
        P(None, "tp"),
        P(None, "tp"),
        P(None, "tp"),
        P("st", "tp"),
    )

    return jax.shard_map(
        body,
        mesh=mesh,
        in_specs=placed,
        out_specs=(P(("st", "tp"), None), P(("st", "tp"), None, None), P(None, "tp")),
        check_vma=False,
    )
```

time: 229 us -> 197 us (0.86)
  waiting for transfers between devices: 106 us -> 64.7 us
  starting transfers between devices: 47.1 us -> 54.3 us
  other arithmetic: 1.65 us -> 4.83 us
  matrix products: 19.4 us -> 16.7 us
  Pallas kernels: 49.3 us -> 51.7 us
    all_to_all x6 -> x7, waiting for transfers between devices: 105 us -> 64.7 us  [exchange(): return lax.all_to_all(x, 'st', split_axis=0, concat_axis=0, tiled=True)]
    all_to_all x6 -> x7, starting transfers between devices: 45.3 us -> 50.9 us  [exchange(): return lax.all_to_all(x, 'st', split_axis=0, concat_axis=0, tiled=True)]
    pallas_call x3 -> x5, Pallas kernels: 17.6 us -> 20.8 us  [the longest x3 16 us: back(): pl.pallas_call(functools.partial(back_kernel, len(terms)), grid=(rows //...]
    convert_element_type x1 -> x2, other arithmetic: 1.55 us -> 4.66 us  [the longest x1 3.11 us: body(): grad_hidden = (keep_hidden + other_hidden.astype(F32)).astype(BF16)]
  transfers between devices with their start and end apart: 13 -> 12, of which waited for: 7 -> 7; matrix products, arithmetic and copies ran while one was open for 9% -> 11% of each run, Pallas kernels for 14% -> 25%
where the time goes in v2:
time: 197 us; the launch traced here: 195 us
  waiting for transfers between devices  64.7 us (33%)
  starting transfers between devices  54.3 us (28%)
  Pallas kernels  51.7 us (26%)
  matrix products  16.7 us (8%)
  other arithmetic  4.83 us (2%)
  local copies, waits for them, and re-layouts  2.21 us (1%)
    all_to_all x7, waiting for transfers between devices, exchange(): return lax.all_to_all(x, 'st', split_axis=0, concat_axis=0, tiled=True)  64.7 us
    all_to_all x7, starting transfers between devices, exchange(): return lax.all_to_all(x, 'st', split_axis=0, concat_axis=0, tiled=True)  50.9 us
    pallas_call x3, Pallas kernels, back(): pl.pallas_call(functools.partial(back_kernel, len(terms)), grid=(rows //...  16 us
    pallas_call x1, Pallas kernels, body(): pl.pallas_call(weight_kernel, grid=(depth // tile,), out_shape=jax.ShapeD...  8.94 us
    dot_general x1, matrix products, body(): jnp.dot(store_rows, key_weight, preferred_element_type=F32).astype(BF16)  6.93 us
    pallas_call x1, Pallas kernels, body(): pl.pallas_call(functools.partial(grads_kernel, held), out_shape=(half_tok...  6.77 us
    dot_general x1, matrix products, body(): jnp.dot(store_rows, value_weight, preferred_element_type=F32).astype(BF16)  6.7 us
    pallas_call x1, Pallas kernels, body(): pl.pallas_call(functools.partial(probs_kernel, held), out_shape=(jax.Shap...  5.42 us
  transfers between devices with their start and end apart: 12, of which 7 were waited for; matrix products, arithmetic and copies ran while one was open for 11% of the time, Pallas kernels for 25%

profile of v2, /device:TPU:0, one launch (start us, length us, event | category | flops | bytes accessed | tf_op | source)
XLA Modules:
  0.0 195.3 jit_solution(11034605046186140304)
XLA Ops:
  0.6 0.0 copy-start
  0.6 0.1 collective-permute-start
  0.7 0.5 collective-permute-start.1
  1.2 1.5 request.1
  2.8 11.5 %all-to-all-start = ((s32[64,1,128]{2,1,0:T(1,128)}), s32[64,1,128]{2,1,0:T(1,128)S(1)}, u32[]{:S(2)}, u32[]{:S(2)}) async-start(s32[64,1,128]{2,1,0:T(1,128)} %bitcast.37), calls=%async_computation | async-start | bytes 65536 | tf_op jit(solution)/shard_map/all_to_all | solution.py:28
  14.3 6.9 %convolution_convert_fusion.1 = bf16[2048,256]{1,0:T(8,128)(2,1)} fusion(bf16[2048,2048]{1,0:T(8,128)(2,1)} %bitcast.25, bf16[2048,256]{1,0:T(8,128)(2,1)} %refs_4_.1), kind=kOutput, calls=%fused_computation.1 | convolution fusion | flops 2148007936 | bytes 10485760 | tf_op jit(solution)/shard_map/dot_general | solution.py:190
  21.2 2.6 %all-to-all-done = s32[64,1,128]{2,1,0:T(1,128)S(1)} async-done(((s32[64,1,128]{2,1,0:T(1,128)}), s32[64,1,128]{2,1,0:T(1,128)S(1)}, u32[]{:S(2)}, u32[]{:S(2)}) %all-to-all-start) | async-done | bytes 32800 | tf_op jit(solution)/shard_map/all_to_all | solution.py:28
  23.8 0.0 copy-start.5
  23.8 0.0 collective-permute-done.refs_0_.refs_5_
  23.8 0.0 copy-start.3
  23.8 0.0 collective-permute-done.1.refs_1_.refs_7_
  23.8 0.6 copy-done.5
  24.4 0.5 copy-done.3
  24.9 2.5 %pick.2 = bf16[64,64,256]{2,1,0:T(8,128)(2,1)} custom-call(s32[64,128]{1,0:T(8,128)} %bitcast.31, s32[1]{0:T(128)S(6)} %mul.11.pause_ref, bf16[32,64,256]{2,1,0:T(8,128)(2,1)} %bitcast.30, bf16[2048,256]{1,0:T(8,128)(2,1)} %copy-done.3, bf16[2048,256]{1,0:T(8,128)(2,1)} %collective-permute-done.1.refs_1_.refs_7_), custom_call_target="tpu_custom_call" | custom-call | tf_op jit(solution)/shard_map/pick/pallas_call | solution.py:56
  27.4 0.0 copy-start.4
  27.5 8.2 %all-to-all-start.1 = ((bf16[64,64,256]{2,1,0:T(8,128)(2,1)}), bf16[64,64,256]{2,1,0:T(8,128)(2,1)}, u32[]{:S(2)}, u32[]{:S(2)}) async-start(bf16[64,64,256]{2,1,0:T(8,128)(2,1)} %pick.2), calls=%async_computation.1 | async-start | bytes 4194304 | tf_op jit(solution)/shard_map/all_to_all | solution.py:28
  35.6 0.0 copy-done.4
  35.6 6.7 %convolution_convert_fusion = bf16[2048,256]{1,0:T(8,128)(2,1)} fusion(bf16[2048,2048]{1,0:T(8,128)(2,1)} %bitcast.26, bf16[2048,256]{1,0:T(8,128)(2,1)S(1)} %copy-done.4), kind=kOutput, calls=%fused_computation | convolution fusion | flops 2148007936 | bytes 10485760 | tf_op jit(solution)/shard_map/dot_general | solution.py:193
  42.3 2.5 %pick.3 = bf16[64,64,256]{2,1,0:T(8,128)(2,1)} custom-call(s32[64,128]{1,0:T(8,128)} %bitcast.32, s32[1]{0:T(128)} %constant.4.clone.1.pause_ref, bf16[32,64,256]{2,1,0:T(8,128)(2,1)} %bitcast.29), custom_call_target="tpu_custom_call" | custom-call | tf_op jit(solution)/shard_map/pick/pallas_call | solution.py:56
  44.9 0.0 copy-start.1
  44.9 11.0 %all-to-all-done.1.k_ref = bf16[64,64,256]{2,1,0:T(8,128)(2,1)} async-done(((bf16[64,64,256]{2,1,0:T(8,128)(2,1)}), bf16[64,64,256]{2,1,0:T(8,128)(2,1)}, u32[]{:S(2)}, u32[]{:S(2)}) %all-to-all-start.1) | async-done | bytes 2097184 | tf_op jit(solution)/shard_map/all_to_all | solution.py:28
  55.9 5.6 %all-to-all-start.3 = ((bf16[64,64,256]{2,1,0:T(8,128)(2,1)}), bf16[64,64,256]{2,1,0:T(8,128)(2,1)}, u32[]{:S(2)}, u32[]{:S(2)}) async-start(bf16[64,64,256]{2,1,0:T(8,128)(2,1)} %pick.3), calls=%async_computation.3 | async-start | bytes 4194304 | tf_op jit(solution)/shard_map/all_to_all | solution.py:28
  61.4 0.0 copy-done
  61.5 0.0 copy-done.1
  61.5 0.0 copy-start.2
  61.5 0.0 copy-start.6
  61.5 1.4 convolution_convert_fusion.2.q_ref
  62.9 0.0 copy-done.2
  62.9 0.0 copy-done.6
  62.9 1.6 multiply_convert_fusion
  64.5 5.4 %probs.1 = (f32[512,256]{1,0:T(8,128)}, bf16[64,64,256]{2,1,0:T(8,128)(2,1)}) custom-call(s32[4,8]{1,0:T(4,128)} %bitcast.39, bf16[512,256]{1,0:T(8,128)(2,1)} %convolution_convert_fusion.2.q_ref, bf16[512,256]{1,0:T(8,128)(2,1)} %get-tuple-element.45.da_ref, bf16[64,64,256]{2,1,0:T(8,128)(2,1)} %all-to-all-done.1.k_ref), custom_call_target="tpu_custom_call" | custom-call | tf_op jit(solution)/shard_map/probs/pallas_call | solution.py:200
  69.9 12.1 %all-to-all-done.3.v_ref = bf16[64,64,256]{2,1,0:T(8,128)(2,1)} async-done(((bf16[64,64,256]{2,1,0:T(8,128)(2,1)}), bf16[64,64,256]{2,1,0:T(8,128)(2,1)}, u32[]{:S(2)}, u32[]{:S(2)}) %all-to-all-start.3) | async-done | bytes 2097184 | tf_op jit(solution)/shard_map/all_to_all | solution.py:28
  82.0 5.7 %all-to-all-start.2 = ((bf16[64,64,256]{2,1,0:T(8,128)(2,1)}), bf16[64,64,256]{2,1,0:T(8,128)(2,1)}, u32[]{:S(2)}, u32[]{:S(2)}) async-start(bf16[64,64,256]{2,1,0:T(8,128)(2,1)} %get-tuple-element.24), calls=%async_computation.2 | async-start | bytes 4194304 | tf_op jit(solution)/shard_map/all_to_all | solution.py:28
  87.8 6.8 %grads.1 = (bf16[256,256]{1,0:T(8,128)(2,1)}, bf16[256,256]{1,0:T(8,128)(2,1)}, bf16[256,256]{1,0:T(8,128)(2,1)}, bf16[256,256]{1,0:T(8,128)(2,1)}, bf16[64,64,256]{2,1,0:T(8,128)(2,1)}) custom-call(s32[4,8]{1,0:T(4,128)} %bitcast.40, s32[1]{0:T(128)} %bitcast.5.tp_ref, bf16[512,256]{1,0:T(8,128)(2,1)} %convolution_convert_fusion.2.q_ref, ...), custom_call_target="tpu_custom_call" | custom-call | tf_op jit(solution)/shard_map/grads/pallas_call | solution.py:214
  94.6 13.7 %all-to-all-done.2.came_ref = bf16[64,64,256]{2,1,0:T(8,128)(2,1)} async-done(((bf16[64,64,256]{2,1,0:T(8,128)(2,1)}), bf16[64,64,256]{2,1,0:T(8,128)(2,1)}, u32[]{:S(2)}, u32[]{:S(2)}) %all-to-all-start.2) | async-done | bytes 2097184 | tf_op jit(solution)/shard_map/all_to_all | solution.py:28
  108.3 7.2 %all-to-all-start.4 = ((bf16[64,64,256]{2,1,0:T(8,128)(2,1)}), bf16[64,64,256]{2,1,0:T(8,128)(2,1)}, u32[]{:S(2)}, u32[]{:S(2)}) async-start(bf16[64,64,256]{2,1,0:T(8,128)(2,1)} %get-tuple-element.27), calls=%async_computation.4 | async-start | bytes 4194304 | tf_op jit(solution)/shard_map/all_to_all | solution.py:28
  115.5 4.7 %value_totals.1 = (bf16[16,64,256]{2,1,0:T(8,128)(2,1)}, bf16[16,64,256]{2,1,0:T(8,128)(2,1)}, bf16[256,2048]{1,0:T(8,128)(2,1)}) custom-call(s32[64,128]{1,0:T(8,128)} %bitcast.33, s32[1]{0:T(128)} %bitcast.5.tp_ref, bf16[64,64,256]{2,1,0:T(8,128)(2,1)} %all-to-all-done.2.came_ref), custom_call_target="tpu_custom_call" | custom-call | tf_op jit(solution)/shard_map/value_totals/pallas_call | solution.py:223
  120.3 8.9 %weight.1 = bf16[64,32,256]{2,1,0:T(8,128)(2,1)} custom-call(bf16[2048,2048]{1,0:T(8,128)(2,1)} %bitcast.27, bf16[256,2048]{1,0:T(8,128)(2,1)} %get-tuple-element.25.vt_ref), custom_call_target="tpu_custom_call" | custom-call | tf_op jit(solution)/shard_map/weight/pallas_call | solution.py:234
  129.2 10.6 %all-to-all-done.4.came_ref = bf16[64,64,256]{2,1,0:T(8,128)(2,1)} async-done(((bf16[64,64,256]{2,1,0:T(8,128)(2,1)}), bf16[64,64,256]{2,1,0:T(8,128)(2,1)}, u32[]{:S(2)}, u32[]{:S(2)}) %all-to-all-start.4) | async-done | bytes 2097184 | tf_op jit(solution)/shard_map/all_to_all | solution.py:28
  139.8 8.0 %all-to-all-start.5 = ((bf16[64,32,256]{2,1,0:T(8,128)(2,1)}), bf16[64,32,256]{2,1,0:T(8,128)(2,1)S(1)}, u32[]{:S(2)}, u32[]{:S(2)}) async-start(bf16[64,32,256]{2,1,0:T(8,128)(2,1)} %weight.1), calls=%async_computation.5 | async-start | bytes 2097152 | tf_op jit(solution)/shard_map/all_to_all | solution.py:28
  147.8 3.4 %back.4 = bf16[256,2048]{1,0:T(8,128)(2,1)} custom-call(bf16[256,256]{1,0:T(8,128)(2,1)} %get-tuple-element.33.refs_0_, bf16[256,256]{1,0:T(8,128)(2,1)} %get-tuple-element.34.refs_1_, bf16[2048,256]{1,0:T(8,128)(2,1)} %refs_2_.3, bf16[2048,256]{1,0:T(8,128)(2,1)} %refs_3_.3), custom_call_target="tpu_custom_call" | custom-call | tf_op jit(solution)/shard_map/back/pallas_call | solution.py:159
  151.2 3.7 %back.3 = f32[256,2048]{1,0:T(8,128)} custom-call(bf16[256,256]{1,0:T(8,128)(2,1)} %get-tuple-element.31.refs_0_, bf16[256,256]{1,0:T(8,128)(2,1)} %get-tuple-element.32.refs_1_, bf16[2048,256]{1,0:T(8,128)(2,1)} %refs_2_.3, bf16[2048,256]{1,0:T(8,128)(2,1)} %refs_3_.3), custom_call_target="tpu_custom_call" | custom-call | tf_op jit(solution)/shard_map/back/pallas_call | solution.py:159
  155.0 3.3 %key_totals.1 = (bf16[16,64,256]{2,1,0:T(8,128)(2,1)}, bf16[16,64,256]{2,1,0:T(8,128)(2,1)}) custom-call(s32[64,128]{1,0:T(8,128)} %bitcast.34, s32[1]{0:T(128)} %bitcast.5.tp_ref, bf16[64,64,256]{2,1,0:T(8,128)(2,1)} %all-to-all-done.4.came_ref), custom_call_target="tpu_custom_call" | custom-call | tf_op jit(solution)/shard_map/key_totals/pallas_call | solution.py:247
  158.3 7.4 %all-to-all-done.5 = bf16[64,32,256]{2,1,0:T(8,128)(2,1)S(1)} async-done(((bf16[64,32,256]{2,1,0:T(8,128)(2,1)}), bf16[64,32,256]{2,1,0:T(8,128)(2,1)S(1)}, u32[]{:S(2)}, u32[]{:S(2)}) %all-to-all-start.5) | async-done | bytes 1048608 | tf_op jit(solution)/shard_map/all_to_all | solution.py:28
  165.6 2.3 %collective-permute-start.2 = (bf16[256,2048]{1,0:T(8,128)(2,1)}, bf16[256,2048]{1,0:T(8,128)(2,1)}, u32[]{:S(2)}, u32[]{:S(2)}) collective-permute-start(bf16[256,2048]{1,0:T(8,128)(2,1)} %back.4), channel_id=1, source_target_pairs={{0,1},{1,0},{2,3},{3,2},{4,5},{5,4},{6,7},{7,6},{8,9},{9,8},{10,11... | collective-permute-start | bytes 3145736 | tf_op jit(solution)/shard_map/ppermute | solution.py:24
  168.0 0.0 collective-permute-start.4
  168.0 0.5 collective-permute-start.3
  168.5 0.2 reduce_sum.12
  168.6 1.1 broadcast_in_dim.3
  169.7 4.7 %all-to-all-start.6 = ((bf16[64,32,256]{2,1,0:T(8,128)(2,1)}), bf16[64,32,256]{2,1,0:T(8,128)(2,1)S(1)}, u32[]{:S(2)}, u32[]{:S(2)}) async-start(bf16[64,32,256]{2,1,0:T(8,128)(2,1)} %broadcast_in_dim.3), calls=%async_computation.6 | async-start | bytes 2097152 | tf_op jit(solution)/shard_map/all_to_all | solution.py:28
  174.4 0.0 collective-permute-done.4.refs_3_
  174.4 0.0 collective-permute-done.3.refs_1_
  174.4 8.9 %back.5 = bf16[1024,2048]{1,0:T(8,128)(2,1)} custom-call(bf16[1024,256]{1,0:T(8,128)(2,1)} %bitcast.36, bf16[1024,256]{1,0:T(8,128)(2,1)} %collective-permute-done.3.refs_1_, bf16[1024,256]{1,0:T(8,128)(2,1)} %bitcast.35, bf16[1024,256]{1,0:T(8,128)(2,1)} %collective-permute-done.4.refs_3_, bf16[2048,256]{1,0:T(8,128)(2,1)} %refs_4_.1, ...), custom_call_target="tpu_custom_call" | custom-call | tf_op jit(solution)/shard_map/back/pallas_call | solution.py:159
  183.3 0.0 collective-permute-done.2
  183.3 3.1 %add_convert_fusion = bf16[256,2048]{1,0:T(8,128)(2,1)} fusion(f32[256,2048]{1,0:T(8,128)} %back.3, bf16[256,2048]{1,0:T(8,128)(2,1)} %collective-permute-done.2), kind=kLoop, calls=%fused_computation.2 | loop fusion | flops 1572864 | bytes 4194304 | tf_op jit(solution)/shard_map/convert_element_type | solution.py:270
  186.4 7.3 %all-to-all-done.6 = bf16[64,32,256]{2,1,0:T(8,128)(2,1)S(1)} async-done(((bf16[64,32,256]{2,1,0:T(8,128)(2,1)}), bf16[64,32,256]{2,1,0:T(8,128)(2,1)S(1)}, u32[]{:S(2)}, u32[]{:S(2)}) %all-to-all-start.6) | async-done | bytes 1048608 | tf_op jit(solution)/shard_map/all_to_all | solution.py:28
  193.7 1.5 bitcast_convert_fusion
Async XLA Ops:
  0.6 60.8 %copy-start = (bf16[512,2048]{1,0:T(8,128)(2,1)S(1)}, bf16[512,2048]{1,0:T(8,128)(2,1)}, u32[]{:S(2)}) copy-start(bf16[512,2048]{1,0:T(8,128)(2,1)} %param.8) | copy-start | bytes 6291460
  0.6 23.2 %collective-permute-start = (bf16[2048,256]{1,0:T(8,128)(2,1)}, bf16[2048,256]{1,0:T(8,128)(2,1)S(1)}, u32[]{:S(2)}, u32[]{:S(2)}) collective-permute-start(bf16[2048,256]{1,0:T(8,128)(2,1)} %refs_4_.1), channel_id=1, source_target_pairs={{0,1},{1,0},{2,3},{3,2},{4,5},{5,4},{6,7},{7,6},{8,9},{9,8},{10,11... | collective-permute-start | bytes 3145736 | tf_op jit(solution)/shard_map/ppermute | solution.py:24
  0.7 23.1 %collective-permute-start.1 = (bf16[2048,256]{1,0:T(8,128)(2,1)}, bf16[2048,256]{1,0:T(8,128)(2,1)}, u32[]{:S(2)}, u32[]{:S(2)}) collective-permute-start(bf16[2048,256]{1,0:T(8,128)(2,1)} %refs_6_.1), channel_id=1, source_target_pairs={{0,1},{1,0},{2,3},{3,2},{4,5},{5,4},{6,7},{7,6},{8,9},{9,8},{10,11... | collective-permute-start | bytes 3145736 | tf_op jit(solution)/shard_map/ppermute | solution.py:24
  2.8 21.0 %all-to-all-start = ((s32[64,1,128]{2,1,0:T(1,128)}), s32[64,1,128]{2,1,0:T(1,128)S(1)}, u32[]{:S(2)}, u32[]{:S(2)}) async-start(s32[64,1,128]{2,1,0:T(1,128)} %bitcast.37), calls=%async_computation | async-start | bytes 65536 | tf_op jit(solution)/shard_map/all_to_all | solution.py:28
  23.8 0.6 copy-start.5
  23.8 1.1 copy-start.3
  27.4 8.2 %copy-start.4 = (bf16[2048,256]{1,0:T(8,128)(2,1)S(1)}, bf16[2048,256]{1,0:T(8,128)(2,1)}, u32[]{:S(2)}) copy-start(bf16[2048,256]{1,0:T(8,128)(2,1)} %refs_6_.1) | copy-start | bytes 3145732
  27.5 28.4 %all-to-all-start.1 = ((bf16[64,64,256]{2,1,0:T(8,128)(2,1)}), bf16[64,64,256]{2,1,0:T(8,128)(2,1)}, u32[]{:S(2)}, u32[]{:S(2)}) async-start(bf16[64,64,256]{2,1,0:T(8,128)(2,1)} %pick.2), calls=%async_computation.1 | async-start | bytes 4194304 | tf_op jit(solution)/shard_map/all_to_all | solution.py:28
  44.9 16.6 %copy-start.1 = (bf16[2048,256]{1,0:T(8,128)(2,1)S(1)}, bf16[2048,256]{1,0:T(8,128)(2,1)}, u32[]{:S(2)}) copy-start(bf16[2048,256]{1,0:T(8,128)(2,1)} %refs_2_.3) | copy-start | bytes 3145732
  55.9 26.2 %all-to-all-start.3 = ((bf16[64,64,256]{2,1,0:T(8,128)(2,1)}), bf16[64,64,256]{2,1,0:T(8,128)(2,1)}, u32[]{:S(2)}, u32[]{:S(2)}) async-start(bf16[64,64,256]{2,1,0:T(8,128)(2,1)} %pick.3), calls=%async_computation.3 | async-start | bytes 4194304 | tf_op jit(solution)/shard_map/all_to_all | solution.py:28
  61.5 1.5 copy-start.2
  61.5 1.4 copy-start.6
  82.0 26.3 %all-to-all-start.2 = ((bf16[64,64,256]{2,1,0:T(8,128)(2,1)}), bf16[64,64,256]{2,1,0:T(8,128)(2,1)}, u32[]{:S(2)}, u32[]{:S(2)}) async-start(bf16[64,64,256]{2,1,0:T(8,128)(2,1)} %get-tuple-element.24), calls=%async_computation.2 | async-start | bytes 4194304 | tf_op jit(solution)/shard_map/all_to_all | solution.py:28
  108.3 31.5 %all-to-all-start.4 = ((bf16[64,64,256]{2,1,0:T(8,128)(2,1)}), bf16[64,64,256]{2,1,0:T(8,128)(2,1)}, u32[]{:S(2)}, u32[]{:S(2)}) async-start(bf16[64,64,256]{2,1,0:T(8,128)(2,1)} %get-tuple-element.27), calls=%async_computation.4 | async-start | bytes 4194304 | tf_op jit(solution)/shard_map/all_to_all | solution.py:28
  139.8 25.8 %all-to-all-start.5 = ((bf16[64,32,256]{2,1,0:T(8,128)(2,1)}), bf16[64,32,256]{2,1,0:T(8,128)(2,1)S(1)}, u32[]{:S(2)}, u32[]{:S(2)}) async-start(bf16[64,32,256]{2,1,0:T(8,128)(2,1)} %weight.1), calls=%async_computation.5 | async-start | bytes 2097152 | tf_op jit(solution)/shard_map/all_to_all | solution.py:28
  165.6 17.7 %collective-permute-start.2 = (bf16[256,2048]{1,0:T(8,128)(2,1)}, bf16[256,2048]{1,0:T(8,128)(2,1)}, u32[]{:S(2)}, u32[]{:S(2)}) collective-permute-start(bf16[256,2048]{1,0:T(8,128)(2,1)} %back.4), channel_id=1, source_target_pairs={{0,1},{1,0},{2,3},{3,2},{4,5},{5,4},{6,7},{7,6},{8,9},{9,8},{10,11... | collective-permute-start | bytes 3145736 | tf_op jit(solution)/shard_map/ppermute | solution.py:24
  168.0 6.4 %collective-permute-start.4 = (bf16[1024,256]{1,0:T(8,128)(2,1)}, bf16[1024,256]{1,0:T(8,128)(2,1)}, u32[]{:S(2)}, u32[]{:S(2)}) collective-permute-start(bf16[1024,256]{1,0:T(8,128)(2,1)} %bitcast.41), channel_id=1, source_target_pairs={{0,1},{1,0},{2,3},{3,2},{4,5},{5,4},{6,7},{7,6},{8,9},{9,8},{10,11... | collective-permute-start | bytes 1572872 | tf_op jit(solution)/shard_map/ppermute | solution.py:24
  168.0 6.4 %collective-permute-start.3 = (bf16[1024,256]{1,0:T(8,128)(2,1)}, bf16[1024,256]{1,0:T(8,128)(2,1)}, u32[]{:S(2)}, u32[]{:S(2)}) collective-permute-start(bf16[1024,256]{1,0:T(8,128)(2,1)} %bitcast.42), channel_id=1, source_target_pairs={{0,1},{1,0},{2,3},{3,2},{4,5},{5,4},{6,7},{7,6},{8,9},{9,8},{10,11... | collective-permute-start | bytes 1572872 | tf_op jit(solution)/shard_map/ppermute | solution.py:24
  169.7 24.0 %all-to-all-start.6 = ((bf16[64,32,256]{2,1,0:T(8,128)(2,1)}), bf16[64,32,256]{2,1,0:T(8,128)(2,1)S(1)}, u32[]{:S(2)}, u32[]{:S(2)}) async-start(bf16[64,32,256]{2,1,0:T(8,128)(2,1)} %broadcast_in_dim.3), calls=%async_computation.6 | async-start | bytes 2097152 | tf_op jit(solution)/shard_map/all_to_all | solution.py:28
